TPU v7x, 128 devices: a whole 4x4x4 slice. The times are simulated.
128 devices in a mesh: sp: 64 (over z, y, x), tp: 2 (over core).
Axes of the slice: x: 4, y: 4, z: 4, core: 2. Of those that a mesh axis runs over, the one named last changes fastest.
Arguments:
- stream: bfloat16 [16384, 2048], P('sp', 'tp'), may hold values from -80 to 80
- norm_gain: float32 [2048], P('tp'), may hold values from 0.1 to 1.9
- cotangent: bfloat16 [16384, 2048], P('sp', 'tp'), may hold values from -16 to 16
- route_weights: float32 [16384, 2], P('sp'), may hold values from 0.1 to 1.5
- routes: int32 [16384, 2], P('sp'), may hold values from 0 to 63, all different within a row; in each aligned block of 256 rows (0 to 255, 256 to 511, ...) at most 16 rows name the same one
- conv_input: bfloat16 [16384, 1024], P('sp', 'tp'), may hold values from -6 to 6
- conv_bgate: bfloat16 [16384, 1024], P('sp', 'tp'), may hold values from -6 to 6
- conv_cgate: bfloat16 [16384, 1024], P('sp', 'tp'), may hold values from -6 to 6
- conv_taps: float32 [3, 1024], P(None, 'tp'), may hold values from -3 to 3
- out_proj: bfloat16 [2048, 1024], P(None, 'tp'), may hold values from -0.1875 to 0.1875
- gate_weight: bfloat16 [64, 2048, 1024], P('sp', None, 'tp'), may hold values from -0.125 to 0.125
- up_weight: bfloat16 [64, 2048, 1024], P('sp', None, 'tp'), may hold values from -0.125 to 0.125
- down_weight: bfloat16 [64, 1024, 2048], P('sp', 'tp'), may hold values from -0.1875 to 0.1875
Outputs:
- stream_grad: bfloat16 [16384, 2048], P('sp', 'tp')
- proj_grad: float32 [2048, 1024], P('sp', 'tp')
- input_grad: bfloat16 [16384, 1024], P('sp', 'tp')
- bgate_grad: bfloat16 [16384, 1024], P('sp', 'tp')
- cgate_grad: bfloat16 [16384, 1024], P('sp', 'tp')
- gate_grad: float32 [64, 2048, 1024], P('sp', None, 'tp')
- up_grad: float32 [64, 2048, 1024], P('sp', None, 'tp')
- down_grad: float32 [64, 1024, 2048], P('sp', 'tp')
Inputs may be any that keep to these rules, and one draw needn't show every extreme that they name: `routes`: the 2 experts of a token differ. Among the tokens of one index of sp, no expert is named more than 16 times, a bound that some block reaches.
All inputs are finite; a program needn't handle non-finite values.
Results may differ from a plain program's by a relative error of at most 0.003.
The roundings to bfloat16 on the way count: a program that leaves them out, or rounds other values in their place, can miss the bound.
Values may be sent and summed in bfloat16 or wider, within the bound.
A program may use at most 128 MiB of HBM per device.

v0:
```python
import jax
import jax.numpy as jnp
from jax import lax
from jax.sharding import Mesh
from jax.sharding import PartitionSpec as P

D = 2048
SP = ("sp_0", "sp_1", "sp_2")


EPSILON = 1e-06


def gathered_total(array, axis):
    return lax.all_gather(array, axis).sum(0)


def side_by_side(arrays, axis, split_dim, concat_dim, along):
    both = jnp.concatenate(arrays, axis=along)
    whole, at, outs = (
        lax.all_to_all(both, axis, split_axis=split_dim, concat_axis=concat_dim, tiled=True),
        0,
        [],
    )
    for a in arrays:
        outs.append(lax.slice_in_dim(whole, at, at + a.shape[along], axis=along))
        at += a.shape[along]
    return tuple(outs)


def sent_together(arrays, axis, dim, along):
    ends, at = ([], 0)
    for a in arrays[:-1]:
        at += a.shape[along]
        ends.append(at)
    both = jnp.concatenate(arrays, axis=along)
    return tuple(jnp.split(lax.all_gather(both, axis, axis=dim, tiled=True), ends, axis=along))


def in_blocks(array, dim, length):
    dims = array.shape
    parts = array.reshape(*dims[:dim], length, dims[dim] // length, *dims[dim + 1 :])
    return jnp.moveaxis(parts, dim, 0)


def sent_and_summed(array, axis, dim):
    parts = in_blocks(array, dim, lax.axis_size(axis))
    arrived = lax.all_to_all(parts, axis, split_axis=0, concat_axis=0, tiled=True)
    return arrived.astype(jnp.float32).sum(axis=0)


def joined_along(parts, dim):
    dims = list(parts.shape[1:])
    dims[dim] *= parts.shape[0]
    return jnp.moveaxis(parts, 0, dim).reshape(dims)


def from_everyone(array, axis):
    copies = jnp.broadcast_to(array, (lax.axis_size(axis), *array.shape))
    return lax.all_to_all(copies, axis, split_axis=0, concat_axis=0, tiled=True)


def gathered_copies(array, axis, dim):
    return joined_along(from_everyone(array, axis), dim)


def shifted(value, axis, steps):
    count = lax.axis_size(axis)
    leading, last = (max(0, -steps), min(count, count - steps))
    return lax.ppermute(value, axis, [(source, source + steps) for source in range(leading, last)])


def sum_by_axis(subtotal, axes):
    for axis in axes:
        subtotal = lax.psum_scatter(subtotal, axis, scatter_dimension=0, tiled=True)
    return subtotal


def slot_matrix(routes, experts, capacity):
    assigned = routes.reshape(-1)
    onehot = (assigned[:, None] == jnp.arange(experts, dtype=jnp.int32)[None, :]).astype(jnp.int32)
    earlier = jnp.cumsum(onehot, axis=0) - onehot
    position = jnp.sum(earlier * onehot, axis=1)
    target = assigned * capacity + position
    places = jnp.arange(experts * capacity, dtype=jnp.int32)
    return (places[:, None] == target[None, :]).astype(jnp.bfloat16)


def select_rows(selector, values):
    return jnp.dot(selector, values, preferred_element_type=jnp.float32).astype(jnp.bfloat16)


def contract_rows(left, right):
    return lax.dot_general(
        left, right, (((0,), (0,)), ((), ())), preferred_element_type=jnp.float32
    )


def contract_cols(left, right):
    return lax.dot_general(
        left, right, (((1,), (1,)), ((), ())), preferred_element_type=jnp.float32
    )


def local(
    stream,
    norm_gain,
    cotangent,
    route_weights,
    routes,
    conv_input,
    conv_bgate,
    conv_cgate,
    conv_taps,
    out_proj,
    gate_weight,
    up_weight,
    down_weight,
):
    experts = lax.axis_size(SP)
    tok_count = stream.shape[0]
    top_count = routes.shape[1]
    capacity = 2 * tok_count * top_count // experts
    stream_float = stream.astype(jnp.float32)
    square_sum = gathered_total(jnp.sum(stream_float * stream_float, axis=1), "tp")
    inverse = lax.rsqrt(square_sum / D + EPSILON)[:, None]
    gain_row = norm_gain[None, :]
    normed = (stream_float * inverse * gain_row).astype(jnp.bfloat16)
    cot_float = cotangent.astype(jnp.float32)
    weighted = (route_weights[:, :, None] * cot_float[:, None, :]).astype(jnp.bfloat16)
    weighted = weighted.reshape(tok_count * top_count, -1)
    selector = slot_matrix(routes, experts, capacity)
    token_select = jnp.sum(selector.reshape(experts * capacity, tok_count, top_count), axis=2)
    send_inputs = select_rows(token_select, normed)
    send_grads = select_rows(selector, weighted)
    half_inputs, half_grads = side_by_side((send_inputs, send_grads), SP, 0, 0, 1)
    recv_inputs, recv_grads = sent_together((half_inputs, half_grads), "tp", 1, 0)
    gate_w = gate_weight[0]
    up_w = up_weight[0]
    down_w = down_weight[0]
    gate_lin = jnp.dot(recv_inputs, gate_w, preferred_element_type=jnp.float32)
    up_lin = jnp.dot(recv_inputs, up_w, preferred_element_type=jnp.float32)
    sigmoid_gate = jax.nn.sigmoid(gate_lin)
    silu_gate = gate_lin * sigmoid_gate
    hidden = (silu_gate * up_lin).astype(jnp.bfloat16)
    down_g = contract_rows(hidden, recv_grads)
    hidden_grad = contract_cols(recv_grads, down_w)
    gate_pre = (
        hidden_grad * up_lin * sigmoid_gate * (1.0 + gate_lin * (1.0 - sigmoid_gate))
    ).astype(jnp.bfloat16)
    up_pre = (hidden_grad * silu_gate).astype(jnp.bfloat16)
    gate_g = contract_rows(recv_inputs, gate_pre)
    up_g = contract_rows(recv_inputs, up_pre)
    partial_value = contract_cols(gate_pre, gate_w) + contract_cols(up_pre, up_w)
    rounded = lax.optimization_barrier(partial_value.astype(jnp.bfloat16))
    summed = sent_and_summed(rounded.astype(jnp.float32).astype(jnp.bfloat16), "tp", 1)
    row_grads = summed.astype(jnp.bfloat16)
    returned = lax.all_to_all(row_grads, SP, split_axis=0, concat_axis=0, tiled=True)
    normed_grad = contract_rows(token_select, returned)
    cross = gathered_total(jnp.sum(stream_float * gain_row * normed_grad, axis=1), "tp")
    stream_grad = (
        cot_float
        + inverse * gain_row * normed_grad
        - stream_float * inverse * inverse * inverse * cross[:, None] / D
    ).astype(jnp.bfloat16)
    grad_whole = gathered_copies(stream_grad, "tp", 1)
    input_float = conv_input.astype(jnp.float32)
    cgate_float = conv_cgate.astype(jnp.float32)
    bgate_float = conv_bgate.astype(jnp.float32)
    rim_rows = shifted(jnp.stack([conv_input[-2:], conv_cgate[-2:]]), SP, 1)
    rim_gated = rim_rows[1].astype(jnp.float32) * rim_rows[0].astype(jnp.float32)
    gated = cgate_float * input_float
    extended = jnp.concatenate([rim_gated, gated], axis=0)
    conv_out = (
        conv_taps[0][None, :] * extended[:-2]
        + conv_taps[1][None, :] * extended[1:-1]
        + conv_taps[2][None, :] * extended[2:]
    )
    mixer_out = (bgate_float * conv_out).astype(jnp.bfloat16)
    proj_grad = sum_by_axis(contract_rows(grad_whole, mixer_out), SP)
    mixer_grad = jnp.dot(grad_whole, out_proj, preferred_element_type=jnp.float32)
    delta = mixer_grad * bgate_float
    next_rim = shifted(delta[:2], SP, -1)
    extended_back = jnp.concatenate([delta, next_rim], axis=0)
    gated_grad = (
        conv_taps[2][None, :] * extended_back[:-2]
        + conv_taps[1][None, :] * extended_back[1:-1]
        + conv_taps[0][None, :] * extended_back[2:]
    )
    bgate_grad = (mixer_grad * conv_out).astype(jnp.bfloat16)
    input_grad = (gated_grad * cgate_float).astype(jnp.bfloat16)
    cgate_grad = (gated_grad * input_float).astype(jnp.bfloat16)
    return (
        stream_grad,
        proj_grad,
        input_grad,
        bgate_grad,
        cgate_grad,
        gate_g[None],
        up_g[None],
        down_g[None],
    )


def solution(mesh):
    finer = Mesh(mesh.devices.reshape(4, 4, 4, mesh.shape["tp"]), ("sp_0", "sp_1", "sp_2", "tp"))
    return jax.shard_map(
        local,
        mesh=finer,
        in_specs=(
            P(SP, "tp"),
            P("tp"),
            P(SP, "tp"),
            P(SP, None),
            P(SP, None),
            P(SP, "tp"),
            P(SP, "tp"),
            P(SP, "tp"),
            P(None, "tp"),
            P(None, "tp"),
            P(SP, None, "tp"),
            P(SP, None, "tp"),
            P(SP, "tp", None),
        ),
        out_specs=(
            P(SP, "tp"),
            P(SP, "tp"),
            P(SP, "tp"),
            P(SP, "tp"),
            P(SP, "tp"),
            P(SP, None, "tp"),
            P(SP, None, "tp"),
            P(SP, "tp", None),
        ),
        check_vma=False,
    )
```

profile of v0, /device:TPU:0, one launch (start us, length us, event | category | flops | bytes accessed | tf_op | source)
XLA Modules:
  0.0 303.7 jit_solution(6799366992860196564)
XLA Ops:
  10.3 2.9 mul.206
  13.2 3.7 %mul.207 = f32[512,1024]{1,0:T(8,128)} reshape(f32[256,2,1024]{2,1,0:T(2,128)} %mul.206) | data formatting | bytes 4194304 | tf_op jit(solution)/shard_map/mul | solution.py:130
  17.9 1.8 all-gather.2
  19.8 3.0 fusion.22
  23.6 2.5 pad_maximum_fusion
  26.1 6.4 %copy.54 = bf16[1024,2048]{1,0:T(8,128)(2,1)} copy(bf16[1024,2048]{0,1:T(8,128)(2,1)} %pad_maximum_fusion) | data formatting | bytes 8388608 | tf_op jit(solution)/shard_map/concatenate | solution.py:19
  32.5 64.4 %all_to_all.34 = bf16[64,16,2048]{2,1,0:T(8,128)(2,1)S(1)} all-to-all(bf16[64,16,2048]{2,1,0:T(8,128)(2,1)} %bitcast.76), channel_id=1, replica_groups=mesh['sp_0'=4,'sp_1'=4,'sp_2'=4,'tp'=2] {'sp_0','sp_1','sp_2'}, dimensions={0} | all-to-all | bytes 8388608 | tf_op jit(solution)/shard_map/all_to_all | solution.py:21
  97.4 2.5 pad_maximum_fusion.1
  99.8 19.3 %all-gather.6.cloned.1.call-done = bf16[2048,2048]{1,0:T(8,128)(2,1)} async-done(((bf16[2048,1024]{1,0:T(8,128)(2,1)}), bf16[2048,2048]{1,0:T(8,128)(2,1)}) %all-gather.6.cloned.1.call-update) | async-done | bytes 8388624 | tf_op jit(solution)/shard_map/all_gather | solution.py:37
  119.2 5.3 %fusion.11 = f32[1024,512]{1,0:T(8,128)S(1)} fusion(bf16[2048,2048]{1,0:T(8,128)(2,1)} %all-gather.6.cloned.1.call-done, bf16[1,2048,512]{2,1,0:T(8,128)(2,1)} %param.24), kind=kOutput, calls=%fused_computation.15 | convolution fusion | flops 2147483648 | bytes 8388608 | tf_op jit(solution)/shard_map/dot_general | solution.py:142
  124.6 2.3 fusion.9
  126.9 3.0 multiply_convert_fusion.1
  130.0 2.4 fusion.13
  132.4 2.4 add_convert_fusion
  135.2 8.2 %all_to_all.35 = bf16[2,1024,1024]{2,1,0:T(8,128)(2,1)} all-to-all(bf16[2,1024,1024]{2,1,0:T(8,128)(2,1)S(1)} %bitcast.77), channel_id=1, replica_groups=mesh['sp_0'=4,'sp_1'=4,'sp_2'=4,'tp'=2] {'tp'}, dimensions={0} | all-to-all | bytes 8388608 | tf_op jit(solution)/shard_map/all_to_all | solution.py:48
  143.4 5.2 %reduce_sum.76 = bf16[1024,1024]{1,0:T(8,128)(2,1)} reduce(bf16[2,1024,1024]{2,1,0:T(8,128)(2,1)} %all_to_all.35, bf16[]{:T(256)} %constant.20.clone.1), dimensions={0}, to_apply=%region_6.7 | reduce | flops 1048576 | bytes 6291458 | tf_op jit(solution)/shard_map/reduce_sum | solution.py:49
  148.6 10.6 %all-to-all-start.2 = ((bf16[64,16,1024]{2,1,0:T(8,128)(2,1)}), bf16[64,16,1024]{2,1,0:T(8,128)(2,1)S(1)}, u32[]{:S(2)}, u32[]{:S(2)}) async-start(bf16[64,16,1024]{2,1,0:T(8,128)(2,1)} %bitcast.8), calls=%async_computation.2 | async-start | bytes 4194304 | tf_op jit(solution)/shard_map/all_to_all | solution.py:158
  159.9 3.5 %collective-permute-start = (bf16[2,2,512]{2,1,0:T(2,128)(2,1)S(1)}, bf16[2,2,512]{2,1,0:T(2,128)(2,1)S(1)}, u32[]{:S(2)}, u32[]{:S(2)}) collective-permute-start(bf16[2,2,512]{2,1,0:T(2,128)(2,1)S(1)} %pad_maximum_fusion.4), channel_id=1, source_target_pairs={{0,2},{2,4},{4,6},{6,8},{8,10},{10,12},{12,14},{14,16},{16,18},{18... | collective-permute-start | bytes 12296 | tf_op jit(solution)/shard_map/ppermute | solution.py:70
  163.4 1.9 convert_multiply_fusion.4
  165.3 16.5 %collective-permute-done = bf16[2,2,512]{2,1,0:T(2,128)(2,1)S(1)} collective-permute-done((bf16[2,2,512]{2,1,0:T(2,128)(2,1)S(1)}, bf16[2,2,512]{2,1,0:T(2,128)(2,1)S(1)}, u32[]{:S(2)}, u32[]{:S(2)}) %collective-permute-start) | collective-permute-done | bytes 4128 | tf_op jit(solution)/shard_map/ppermute | solution.py:70
  181.8 7.8 %all-to-all-done.2 = bf16[64,16,1024]{2,1,0:T(8,128)(2,1)S(1)} async-done(((bf16[64,16,1024]{2,1,0:T(8,128)(2,1)}), bf16[64,16,1024]{2,1,0:T(8,128)(2,1)S(1)}, u32[]{:S(2)}, u32[]{:S(2)}) %all-to-all-start.2) | async-done | bytes 2097184 | tf_op jit(solution)/shard_map/all_to_all | solution.py:158
  189.6 1.7 fusion.33
  191.3 1.8 all-gather.3
  193.2 1.8 fusion.30
  195.3 4.7 %all_to_all.36 = bf16[2,256,1024]{1,2,0:T(8,128)(2,1)S(1)} all-to-all(bf16[2,256,1024]{1,2,0:T(8,128)(2,1)S(1)} %broadcast_in_dim.8), channel_id=1, replica_groups=mesh['sp_0'=4,'sp_1'=4,'sp_2'=4,'tp'=2] {'tp'}, dimensions={0} | all-to-all | bytes 2097152 | tf_op jit(solution)/shard_map/all_to_all | solution.py:60
  201.6 2.7 fusion.54
  204.4 43.7 %reduce-scatter.4.cloned.1.call-done = f32[512,512]{1,0:T(8,128)} async-done(((f32[2048,512]{1,0:T(8,128)}), f32[512,512]{1,0:T(8,128)}) %reduce-scatter.4.cloned.1.call-update) | async-done | bytes 1048592 | tf_op jit(solution)/shard_map/reduce_scatter | solution.py:75
  248.2 6.7 %convolution_bitcast_fusion = f32[1,2048,512]{2,1,0:T(8,128)} fusion(bf16[1024,512]{1,0:T(8,128)(2,1)S(1)} %copy-done.17, bf16[2048,2048]{1,0:T(8,128)(2,1)} %all-gather.6.cloned.1.call-done), kind=kOutput, calls=%fused_computation.9 | convolution fusion | flops 2147483648 | bytes 9437184 | tf_op jit(solution)/shard_map/dot_general | solution.py:94
  254.9 6.7 %fusion.4 = f32[1,512,2048]{2,1,0:T(8,128)} fusion(bf16[2048,2048]{1,0:T(8,128)(2,1)} %all-gather.6.cloned.1.call-done, f32[1024,512]{1,0:T(8,128)S(1)} %copy-done.20, f32[1024,512]{1,0:T(8,128)S(1)} %copy-done.22), kind=kOutput, calls=%fused_computation.8 | convolution fusion | flops 2150629376 | bytes 12582912 | tf_op jit(solution)/shard_map/dot_general | solution.py:94
  263.1 10.7 %reduce-scatter.6.cloned.1.call-done = f32[128,512]{1,0:T(8,128)} async-done(((f32[512,512]{1,0:T(8,128)}), f32[128,512]{1,0:T(8,128)}) %reduce-scatter.6.cloned.1.call-update) | async-done | bytes 262160 | tf_op jit(solution)/shard_map/reduce_scatter | solution.py:75
  273.9 7.0 %convolution_bitcast_fusion.1 = f32[1,2048,512]{2,1,0:T(8,128)} fusion(bf16[1024,512]{1,0:T(8,128)(2,1)} %copy-done.18, bf16[2048,2048]{1,0:T(8,128)(2,1)} %all-gather.6.cloned.1.call-done), kind=kOutput, calls=%fused_computation.10 | convolution fusion | flops 2147483648 | bytes 9437184 | tf_op jit(solution)/shard_map/dot_general | solution.py:94
  282.6 14.5 %reduce-scatter.8.cloned.1.call-done = f32[32,512]{1,0:T(8,128)} async-done(((f32[128,512]{1,0:T(8,128)}), f32[32,512]{1,0:T(8,128)}) %reduce-scatter.8.cloned.1.call-update) | async-done | bytes 65552 | tf_op jit(solution)/shard_map/reduce_scatter | solution.py:75
  (89 shorter events, 11.9 us)
Async XLA Ops:
  7.2 117.4 %copy-start = (bf16[1,2048,512]{2,1,0:T(8,128)(2,1)S(1)}, bf16[1,2048,512]{2,1,0:T(8,128)(2,1)}, u32[]{:S(2)}) copy-start(bf16[1,2048,512]{2,1,0:T(8,128)(2,1)} %param.23) | copy-start | bytes 6291460
  7.2 112.0 %all-gather.6.cloned.1.call-start = ((), (), s32[]{:S(2)}) async-start(), calls=%async_computation.7 | async-start | bytes 12582912 | tf_op jit(solution)/shard_map/all_gather | solution.py:37
  13.2 3.7 %copy-start.12 = (f32[256,2]{0,1:T(2,128)S(1)}, f32[256,2]{0,1:T(2,128)}, u32[]{:S(2)}) copy-start(f32[256,2]{0,1:T(2,128)} %param.16) | copy-start | bytes 6148
  13.2 4.1 %copy-start.10 = (s32[256,2]{0,1:T(2,128)S(1)}, s32[256,2]{0,1:T(2,128)}, u32[]{:S(2)}) copy-start(s32[256,2]{0,1:T(2,128)} %param.17) | copy-start | bytes 6148
  13.2 4.6 %copy-start.2 = (bf16[256,1024]{1,0:T(8,128)(2,1)S(1)}, bf16[256,1024]{1,0:T(8,128)(2,1)}, u32[]{:S(2)}) copy-start(bf16[256,1024]{1,0:T(8,128)(2,1)} %param.13) | copy-start | bytes 1572868
  19.8 3.0 copy-start.9
  119.2 5.3 %copy-start.13 = (bf16[2048,2048]{1,0:T(8,128)(2,1)S(1)}, bf16[2048,2048]{1,0:T(8,128)(2,1)}, u32[]{:S(2)}) copy-start(bf16[2048,2048]{1,0:T(8,128)(2,1)} %all-gather.6.cloned.1.call-done) | copy-start | bytes 25165828
  124.5 2.3 copy-start.19
  124.5 2.4 copy-start.14
  126.9 3.0 copy-start.21
  129.9 2.4 copy-start.18
  130.0 2.4 copy-start.16
  130.0 2.4 copy-start.15
  148.6 10.6 %copy-start.6 = (bf16[256,512]{1,0:T(8,128)(2,1)S(1)}, bf16[256,512]{1,0:T(8,128)(2,1)}, u32[]{:S(2)}) copy-start(bf16[256,512]{1,0:T(8,128)(2,1)} %param.18) | copy-start | bytes 786436
  148.6 16.7 %copy-start.11 = (f32[3,512]{1,0:T(4,128)S(1)}, f32[3,512]{1,0:T(4,128)}, u32[]{:S(2)}) copy-start(f32[3,512]{1,0:T(4,128)} %param.21) | copy-start | bytes 18436
  148.6 41.1 %all-to-all-start.2 = ((bf16[64,16,1024]{2,1,0:T(8,128)(2,1)}), bf16[64,16,1024]{2,1,0:T(8,128)(2,1)S(1)}, u32[]{:S(2)}, u32[]{:S(2)}) async-start(bf16[64,16,1024]{2,1,0:T(8,128)(2,1)} %bitcast.8), calls=%async_computation.2 | async-start | bytes 4194304 | tf_op jit(solution)/shard_map/all_to_all | solution.py:158
  159.1 89.0 %reduce-scatter.4.cloned.1.call-start = ((), (), s32[]{:S(2)}) async-start(), calls=%async_computation.8 | async-start | bytes 5242880 | tf_op jit(solution)/shard_map/reduce_scatter | solution.py:75
  159.9 21.9 %collective-permute-start = (bf16[2,2,512]{2,1,0:T(2,128)(2,1)S(1)}, bf16[2,2,512]{2,1,0:T(2,128)(2,1)S(1)}, u32[]{:S(2)}, u32[]{:S(2)}) collective-permute-start(bf16[2,2,512]{2,1,0:T(2,128)(2,1)S(1)} %pad_maximum_fusion.4), channel_id=1, source_target_pairs={{0,2},{2,4},{4,6},{6,8},{8,10},{10,12},{12,14},{14,16},{16,18},{18... | collective-permute-start | bytes 12296 | tf_op jit(solution)/shard_map/ppermute | solution.py:70
  195.0 5.0 %copy-start.5 = (bf16[256,1024]{1,0:T(8,128)(2,1)}, bf16[256,1024]{1,0:T(8,128)(2,1)S(1)}, u32[]{:S(2)}) copy-start(bf16[256,1024]{1,0:T(8,128)(2,1)S(1)} %fusion.30) | copy-start | bytes 1572868
  195.2 4.8 %copy-start.3 = (f32[256,512]{1,0:T(8,128)S(1)}, f32[256,512]{1,0:T(8,128)}, u32[]{:S(2)}) copy-start(f32[256,512]{1,0:T(8,128)} %convert_multiply_fusion.4) | copy-start | bytes 1572868
  195.2 4.8 %copy-start.4 = (bf16[2048,512]{1,0:T(8,128)(2,1)S(1)}, bf16[2048,512]{1,0:T(8,128)(2,1)}, u32[]{:S(2)}) copy-start(bf16[2048,512]{1,0:T(8,128)(2,1)} %param.22) | copy-start | bytes 6291460
  195.2 4.8 %copy-start.8 = (bf16[256,512]{1,0:T(8,128)(2,1)S(1)}, bf16[256,512]{1,0:T(8,128)(2,1)}, u32[]{:S(2)}) copy-start(bf16[256,512]{1,0:T(8,128)(2,1)} %param.19) | copy-start | bytes 786436
  204.3 43.8 %copy-start.17 = (bf16[1024,512]{1,0:T(8,128)(2,1)S(1)}, bf16[1024,512]{1,0:T(8,128)(2,1)}, u32[]{:S(2)}) copy-start(bf16[1024,512]{1,0:T(8,128)(2,1)} %copy-done.16) | copy-start | bytes 3145732
  204.3 69.5 %reduce-scatter.6.cloned.1.call-start = ((), (), s32[]{:S(2)}) async-start(), calls=%async_computation.9 | async-start | bytes 1310720 | tf_op jit(solution)/shard_map/reduce_scatter | solution.py:75
  248.1 49.0 %reduce-scatter.8.cloned.1.call-start = ((), (), s32[]{:S(2)}) async-start(), calls=%async_computation.10 | async-start | bytes 327680 | tf_op jit(solution)/shard_map/reduce_scatter | solution.py:75
  248.2 6.8 %copy-start.20 = (f32[1024,512]{1,0:T(8,128)S(1)}, f32[1024,512]{1,0:T(8,128)}, u32[]{:S(2)}) copy-start(f32[1024,512]{1,0:T(8,128)} %copy-done.19) | copy-start | bytes 6291460
  248.2 6.7 %copy-start.22 = (f32[1024,512]{1,0:T(8,128)S(1)}, f32[1024,512]{1,0:T(8,128)}, u32[]{:S(2)}) copy-start(f32[1024,512]{1,0:T(8,128)} %copy-done.21) | copy-start | bytes 6291460
  261.6 19.3 %collective-permute-start.1 = (f32[2,512]{1,0:T(2,128)S(1)}, f32[2,512]{1,0:T(2,128)S(1)}, u32[]{:S(2)}, u32[]{:S(2)}) collective-permute-start(f32[2,512]{1,0:T(2,128)S(1)} %slice.74), channel_id=1, source_target_pairs={{2,0},{4,2},{6,4},{8,6},{10,8},{12,10},{14,12},{16,14},{18,16},{20... | collective-permute-start | bytes 12296 | tf_op jit(solution)/shard_map/ppermute | solution.py:70
  273.9 8.0 %copy-start.7 = (bf16[256,512]{1,0:T(8,128)(2,1)S(1)}, bf16[256,512]{1,0:T(8,128)(2,1)}, u32[]{:S(2)}) copy-start(bf16[256,512]{1,0:T(8,128)(2,1)} %param.20) | copy-start | bytes 786436
  273.9 23.3 %copy-start.1 = (bf16[1,2048,512]{2,1,0:T(8,128)(2,1)S(1)}, bf16[1,2048,512]{2,1,0:T(8,128)(2,1)}, u32[]{:S(2)}) copy-start(bf16[1,2048,512]{2,1,0:T(8,128)(2,1)} %param.23) | copy-start | bytes 6291460
Sparse Core Ops, SparseCore 0:
  100.0 19.1 all-gather.5
  204.5 43.5 reduce-scatter.3
  250.5 23.2 reduce-scatter.5
  276.6 20.4 reduce-scatter.7
where the time goes:
time: 305 us; the launch traced here: 304 us
  waiting for transfers between devices  113 us (37%)
  blocking collectives  80.9 us (27%)
  matrix products  45.6 us (15%)
  other arithmetic  17.5 us (6%)
  local copies, waits for them, and re-layouts  17 us (6%)
  starting transfers between devices  15.7 us (5%)
  between operations  14.2 us (5%)
    reduce_scatter x3, waiting for transfers between devices, sum_by_axis(): subtotal = lax.psum_scatter(subtotal, axis, scatter_dimension=0, tiled=True)  69 us
    all_to_all x1, blocking collectives, side_by_side(): lax.all_to_all(both, axis, split_axis=split_dim, concat_axis=concat_dim,...  64.4 us
    dot_general x5, matrix products, contract_rows(): lax.dot_general(left, right, (((0,), (0,)), ((), ())), preferred_element_...  24.9 us
    all_gather x1, waiting for transfers between devices, sent_together(): lax.all_gather(both, axis, axis=dim, tiled=True)  19.3 us
    ppermute x2, waiting for transfers between devices, shifted(): lax.ppermute(value, axis, [(source, source + steps) for source in range(l...  16.6 us
    all_to_all x1, starting transfers between devices, local(): lax.all_to_all(row_grads, SP, split_axis=0, concat_axis=0, tiled=True)  10.6 us
    all_to_all x1, blocking collectives, sent_and_summed(): lax.all_to_all(parts, axis, split_axis=0, concat_axis=0, tiled=True)  8.18 us
    all_to_all x1, waiting for transfers between devices, local(): lax.all_to_all(row_grads, SP, split_axis=0, concat_axis=0, tiled=True)  7.83 us
  transfers between devices with their start and end apart: 7, of which 6 were waited for; matrix products, arithmetic and copies ran while one was open for 8% of the time, Pallas kernels for 0%

commit v1 on v0

v1 whole, which is shorter than its diff:
```python
import functools

import jax
import jax.numpy as jnp
from jax import lax
from jax.experimental import pallas as pl
from jax.experimental.pallas import tpu as pltpu
from jax.sharding import PartitionSpec as P

D = 2048
EPSILON = 1e-06
MESH = pl.DeviceIdType.MESH
SIDE = 4
CHIPS = SIDE**3


def _parts(k):
    return k // 16, (k // 4) % 4, k % 4


def _join(z, y, x):
    return (z % 4) * 16 + (y % 4) * 4 + x % 4


def _shift_order():
    hops = lambda k: sum(min(a, SIDE - a) for a in _parts(k))
    turn = lambda k: _join(*(_parts(k)[1:] + _parts(k)[:1]))
    back = lambda k: _join(*(-a for a in _parts(k)))
    order = []
    for k in sorted(range(1, CHIPS), key=lambda k: -hops(k)):
        for kk in (k, turn(k), turn(turn(k))):
            for other in (kk,):
                if other not in order:
                    order.append(other)
        for kk in (k, turn(k), turn(turn(k))):
            if back(kk) not in order:
                order.append(back(kk))
    return order


ORDER = _shift_order()


def moved(me, k, sign=1):
    z, y, x = me // 16, lax.rem(me // 4, 4), lax.rem(me, 4)
    kz, ky, kx = (a if sign > 0 else (SIDE - a) % SIDE for a in _parts(k))
    return lax.rem(z + kz, 4) * 16 + lax.rem(y + ky, 4) * 4 + lax.rem(x + kx, 4)


def greet_all(me, core, partner):
    barrier = pltpu.get_barrier_semaphore()
    for k in ORDER:
        pl.semaphore_signal(
            barrier, inc=1, device_id=(moved(me, k), core), device_id_type=MESH
        )
    count = CHIPS - 1
    if partner:
        pl.semaphore_signal(barrier, inc=1, device_id=(me, 1 - core), device_id_type=MESH)
        count += 1
    pl.semaphore_wait(barrier, count)


def dispatch_kernel(group, send, out, send_sem, recv_sem, pass_send, pass_recv):
    me, core = lax.axis_index("sp"), lax.axis_index("tp")
    greet_all(me, core, True)
    copies = []
    for j, k in enumerate(ORDER):
        peer = moved(me, k)
        copy = pltpu.make_async_remote_copy(
            src_ref=send.at[peer],
            dst_ref=out.at[core, j],
            send_sem=send_sem.at[j],
            recv_sem=recv_sem.at[j],
            device_id=(peer, core),
            device_id_type=MESH,
        )
        copy.start()
        copies.append(copy)
    out[core, CHIPS - 1] = send[me]
    passes = []
    for g in range(CHIPS // group):
        for j in range(g * group, (g + 1) * group):
            if j < CHIPS - 1:
                copies[j].wait_recv()
        onward = pltpu.make_async_remote_copy(
            src_ref=out.at[core, pl.ds(g * group, group)],
            dst_ref=out.at[core, pl.ds(g * group, group)],
            send_sem=pass_send.at[g],
            recv_sem=pass_recv.at[g],
            device_id=(me, 1 - core),
            device_id_type=MESH,
        )
        onward.start()
        passes.append(onward)
    for onward in passes:
        onward.wait()
    for copy in copies:
        copy.wait_send()


def dispatch(send):
    rows, columns = send.shape[1:]
    group = 8
    vmem = pl.BlockSpec(memory_space=pltpu.VMEM)
    return pl.pallas_call(
        functools.partial(dispatch_kernel, group),
        out_shape=jax.ShapeDtypeStruct((2, CHIPS, rows, columns), send.dtype),
        in_specs=[vmem],
        out_specs=vmem,
        scratch_shapes=[
            pltpu.SemaphoreType.DMA((CHIPS,)),
            pltpu.SemaphoreType.DMA((CHIPS,)),
            pltpu.SemaphoreType.DMA((CHIPS // group,)),
            pltpu.SemaphoreType.DMA((CHIPS // group,)),
        ],
        compiler_params=pltpu.CompilerParams(
            collective_id=0, has_side_effects=True, vmem_limit_bytes=40 << 20
        ),
        name="dispatch",
    )(send)


def swap_kernel(backward, send, out, send_sem, recv_sem):
    me, core = lax.axis_index("sp"), lax.axis_index("tp")
    greet_all(me, core, False)
    copies = []
    for j, k in enumerate(ORDER):
        peer = moved(me, k, -1 if backward else 1)
        copy = pltpu.make_async_remote_copy(
            src_ref=send.at[j if backward else peer],
            dst_ref=out.at[me if backward else j],
            send_sem=send_sem.at[j],
            recv_sem=recv_sem.at[j],
            device_id=(peer, core),
            device_id_type=MESH,
        )
        copy.start()
        copies.append(copy)
    if backward:
        out[me] = send[CHIPS - 1]
    else:
        out[CHIPS - 1] = send[me]
    for copy in copies:
        copy.wait()


def swap(send, backward, collective_id, name):
    vmem = pl.BlockSpec(memory_space=pltpu.VMEM)
    return pl.pallas_call(
        functools.partial(swap_kernel, backward),
        out_shape=jax.ShapeDtypeStruct(send.shape, send.dtype),
        in_specs=[vmem],
        out_specs=vmem,
        scratch_shapes=[
            pltpu.SemaphoreType.DMA((CHIPS,)),
            pltpu.SemaphoreType.DMA((CHIPS,)),
        ],
        compiler_params=pltpu.CompilerParams(
            collective_id=collective_id, has_side_effects=True, vmem_limit_bytes=24 << 20
        ),
        name=name,
    )(send)


def gathered_total(array, axis):
    return lax.all_gather(array, axis).sum(0)


def sent_and_summed(array, axis, dim):
    dims = array.shape
    length = lax.axis_size(axis)
    parts = array.reshape(*dims[:dim], length, dims[dim] // length, *dims[dim + 1 :])
    parts = jnp.moveaxis(parts, dim, 0)
    arrived = lax.all_to_all(parts, axis, split_axis=0, concat_axis=0, tiled=True)
    return arrived.astype(jnp.float32).sum(axis=0)


def gathered_copies(array, axis, dim):
    copies = jnp.broadcast_to(array, (lax.axis_size(axis), *array.shape))
    parts = lax.all_to_all(copies, axis, split_axis=0, concat_axis=0, tiled=True)
    return jnp.concatenate([parts[0], parts[1]], axis=dim)


def shifted(value, axis, steps):
    count = lax.axis_size(axis)
    leading, last = (max(0, -steps), min(count, count - steps))
    return lax.ppermute(value, axis, [(source, source + steps) for source in range(leading, last)])


def slot_matrix(routes, experts, capacity):
    assigned = routes.reshape(-1)
    onehot = (assigned[:, None] == jnp.arange(experts, dtype=jnp.int32)[None, :]).astype(jnp.int32)
    earlier = jnp.cumsum(onehot, axis=0) - onehot
    position = jnp.sum(earlier * onehot, axis=1)
    target = assigned * capacity + position
    places = jnp.arange(experts * capacity, dtype=jnp.int32)
    return (places[:, None] == target[None, :]).astype(jnp.bfloat16)


def select_rows(selector, values):
    return jnp.dot(selector, values, preferred_element_type=jnp.float32).astype(jnp.bfloat16)


def contract_rows(left, right):
    return lax.dot_general(
        left, right, (((0,), (0,)), ((), ())), preferred_element_type=jnp.float32
    )


def contract_cols(left, right):
    return lax.dot_general(
        left, right, (((1,), (1,)), ((), ())), preferred_element_type=jnp.float32
    )


def local(
    stream,
    norm_gain,
    cotangent,
    route_weights,
    routes,
    conv_input,
    conv_bgate,
    conv_cgate,
    conv_taps,
    out_proj,
    gate_weight,
    up_weight,
    down_weight,
):
    experts = lax.axis_size("sp")
    tok_count = stream.shape[0]
    top_count = routes.shape[1]
    capacity = 2 * tok_count * top_count // experts
    half = stream.shape[1]
    stream_float = stream.astype(jnp.float32)
    square_sum = gathered_total(jnp.sum(stream_float * stream_float, axis=1), "tp")
    inverse = lax.rsqrt(square_sum / D + EPSILON)[:, None]
    gain_row = norm_gain[None, :]
    normed = (stream_float * inverse * gain_row).astype(jnp.bfloat16)
    cot_float = cotangent.astype(jnp.float32)
    weighted = (route_weights[:, :, None] * cot_float[:, None, :]).astype(jnp.bfloat16)
    weighted = weighted.reshape(tok_count * top_count, -1)
    selector = slot_matrix(routes, experts, capacity)
    token_select = jnp.sum(selector.reshape(experts * capacity, tok_count, top_count), axis=2)
    send_inputs = select_rows(token_select, normed)
    send_grads = select_rows(selector, weighted)
    send = jnp.concatenate([send_inputs, send_grads], axis=1)
    arrived = dispatch(send.reshape(experts, capacity, 2 * half))
    arrived = arrived.reshape(2, experts * capacity, 2 * half)
    recv_inputs = jnp.concatenate([arrived[0, :, :half], arrived[1, :, :half]], axis=1)
    recv_grads = jnp.concatenate([arrived[0, :, half:], arrived[1, :, half:]], axis=1)
    gate_w = gate_weight[0]
    up_w = up_weight[0]
    down_w = down_weight[0]
    gate_lin = jnp.dot(recv_inputs, gate_w, preferred_element_type=jnp.float32)
    up_lin = jnp.dot(recv_inputs, up_w, preferred_element_type=jnp.float32)
    sigmoid_gate = jax.nn.sigmoid(gate_lin)
    silu_gate = gate_lin * sigmoid_gate
    hidden = (silu_gate * up_lin).astype(jnp.bfloat16)
    down_g = contract_rows(hidden, recv_grads)
    hidden_grad = contract_cols(recv_grads, down_w)
    gate_pre = (
        hidden_grad * up_lin * sigmoid_gate * (1.0 + gate_lin * (1.0 - sigmoid_gate))
    ).astype(jnp.bfloat16)
    up_pre = (hidden_grad * silu_gate).astype(jnp.bfloat16)
    gate_g = contract_rows(recv_inputs, gate_pre)
    up_g = contract_rows(recv_inputs, up_pre)
    partial_value = contract_cols(gate_pre, gate_w) + contract_cols(up_pre, up_w)
    rounded = lax.optimization_barrier(partial_value.astype(jnp.bfloat16))
    summed = sent_and_summed(rounded.astype(jnp.float32).astype(jnp.bfloat16), "tp", 1)
    row_grads = summed.astype(jnp.bfloat16)
    returned = swap(row_grads.reshape(experts, capacity, half), True, 1, "give_back")
    returned = returned.reshape(experts * capacity, half)
    normed_grad = contract_rows(token_select, returned)
    cross = gathered_total(jnp.sum(stream_float * gain_row * normed_grad, axis=1), "tp")
    stream_grad = (
        cot_float
        + inverse * gain_row * normed_grad
        - stream_float * inverse * inverse * inverse * cross[:, None] / D
    ).astype(jnp.bfloat16)
    grad_whole = gathered_copies(stream_grad, "tp", 1)
    input_float = conv_input.astype(jnp.float32)
    cgate_float = conv_cgate.astype(jnp.float32)
    bgate_float = conv_bgate.astype(jnp.float32)
    rim_rows = shifted(jnp.stack([conv_input[-2:], conv_cgate[-2:]]), "sp", 1)
    rim_gated = rim_rows[1].astype(jnp.float32) * rim_rows[0].astype(jnp.float32)
    gated = cgate_float * input_float
    extended = jnp.concatenate([rim_gated, gated], axis=0)
    conv_out = (
        conv_taps[0][None, :] * extended[:-2]
        + conv_taps[1][None, :] * extended[1:-1]
        + conv_taps[2][None, :] * extended[2:]
    )
    mixer_out = (bgate_float * conv_out).astype(jnp.bfloat16)
    shares = contract_rows(grad_whole, mixer_out).astype(jnp.bfloat16)
    shares = swap(shares.reshape(experts, D // experts, -1), False, 2, "share")
    proj_grad = shares.astype(jnp.float32).sum(axis=0)
    mixer_grad = jnp.dot(grad_whole, out_proj, preferred_element_type=jnp.float32)
    delta = mixer_grad * bgate_float
    next_rim = shifted(delta[:2], "sp", -1)
    extended_back = jnp.concatenate([delta, next_rim], axis=0)
    gated_grad = (
        conv_taps[2][None, :] * extended_back[:-2]
        + conv_taps[1][None, :] * extended_back[1:-1]
        + conv_taps[0][None, :] * extended_back[2:]
    )
    bgate_grad = (mixer_grad * conv_out).astype(jnp.bfloat16)
    input_grad = (gated_grad * cgate_float).astype(jnp.bfloat16)
    cgate_grad = (gated_grad * input_float).astype(jnp.bfloat16)
    return (
        stream_grad,
        proj_grad,
        input_grad,
        bgate_grad,
        cgate_grad,
        gate_g[None],
        up_g[None],
        down_g[None],
    )


def solution(mesh):
    return jax.shard_map(
        local,
        mesh=mesh,
        in_specs=(
            P("sp", "tp"),
            P("tp"),
            P("sp", "tp"),
            P("sp", None),
            P("sp", None),
            P("sp", "tp"),
            P("sp", "tp"),
            P("sp", "tp"),
            P(None, "tp"),
            P(None, "tp"),
            P("sp", None, "tp"),
            P("sp", None, "tp"),
            P("sp", "tp", None),
        ),
        out_specs=(
            P("sp", "tp"),
            P("sp", "tp"),
            P("sp", "tp"),
            P("sp", "tp"),
            P("sp", "tp"),
            P("sp", None, "tp"),
            P("sp", None, "tp"),
            P("sp", "tp", None),
        ),
        check_vma=False,
    )
```

time: 305 us -> 221 us (0.72)
  Pallas kernels: 0 us -> 129 us
  waiting for transfers between devices: 113 us -> 0.01 us
  blocking collectives: 80.9 us -> 11.8 us
  between operations: 14.2 us -> 1.18 us
  matrix products: 45.6 us -> 36.4 us
  starting transfers between devices: 15.7 us -> 7.78 us
  other arithmetic: 17.5 us -> 11.8 us
  local copies, waits for them, and re-layouts: 17 us -> 22 us
    pallas_call x0 -> x3, Pallas kernels: none -> 129 us  [the longest x2 67.7 us: swap(): pl.pallas_call(functools.partial(swap_kernel, backward), out_shape=jax.Sh...]
    all_to_all x2 -> x0, blocking collectives: 69.1 us -> none  [the longest x1 64.4 us: side_by_side(): lax.all_to_all(both, axis, split_axis=split_dim, concat_axis=concat_dim,...]
    reduce_scatter x3 -> x0, waiting for transfers between devices: 69 us -> none  [sum_by_axis(): subtotal = lax.psum_scatter(subtotal, axis, scatter_dimension=0, tiled=True)]
    all_gather x1 -> x0, waiting for transfers between devices: 19.3 us -> none  [sent_together(): lax.all_gather(both, axis, axis=dim, tiled=True)]
    ppermute x2, waiting for transfers between devices: 16.6 us -> 0.01 us  [shifted(): lax.ppermute(value, axis, [(source, source + steps) for source in range(l...]
    all_to_all x1, waiting for transfers between devices: 7.83 us -> 0.01 us  [gathered_copies(): lax.all_to_all(copies, axis, split_axis=0, concat_axis=0, tiled=True)]
    all_to_all x1, starting transfers between devices: 10.6 us -> 3.58 us  [gathered_copies(): lax.all_to_all(copies, axis, split_axis=0, concat_axis=0, tiled=True)]
    dot_general x5, matrix products: 24.9 us -> 18.5 us  [contract_rows(): lax.dot_general(left, right, (((0,), (0,)), ((), ())), preferred_element_...]
  transfers between devices with their start and end apart: 7 -> 3, of which waited for: 6 -> 0; matrix products, arithmetic and copies ran while one was open for 8% -> 9% of each run, Pallas kernels for 0% -> 16%
where the time goes in v1:
time: 221 us; the launch traced here: 220 us
  Pallas kernels  129 us (58%)
  matrix products  36.4 us (16%)
  local copies, waits for them, and re-layouts  22 us (10%)
  other arithmetic  11.8 us (5%)
  blocking collectives  11.8 us (5%)
  starting transfers between devices  7.78 us (4%)
    pallas_call x2, Pallas kernels, swap(): pl.pallas_call(functools.partial(swap_kernel, backward), out_shape=jax.Sh...  67.7 us
    pallas_call x1, Pallas kernels, dispatch(): pl.pallas_call(functools.partial(dispatch_kernel, group), out_shape=jax.S...  61.2 us
    dot_general x5, matrix products, contract_rows(): lax.dot_general(left, right, (((0,), (0,)), ((), ())), preferred_element_...  18.5 us
    all_to_all x1, blocking collectives, sent_and_summed(): lax.all_to_all(parts, axis, split_axis=0, concat_axis=0, tiled=True)  8.22 us
    dot_general x3, matrix products, contract_cols(): lax.dot_general(left, right, (((1,), (1,)), ((), ())), preferred_element_...  7.92 us
    mul x3, local copies, waits for them, and re-layouts, local(): route_weights[:, :, None] * cot_float[:, None, :]  6.76 us
    concatenate x1, local copies, waits for them, and re-layouts, local(): send = jnp.concatenate([send_inputs, send_grads], axis=1)  6.42 us
    unnamed x58, local copies, waits for them, and re-layouts  5.49 us
  transfers between devices with their start and end apart: 3, of which 0 were waited for; matrix products, arithmetic and copies ran while one was open for 9% of the time, Pallas kernels for 16%

profile of v1, /device:TPU:0, one launch (start us, length us, event | category | flops | bytes accessed | tf_op | source)
XLA Modules:
  0.0 219.9 jit_solution(14942670795830479159)
XLA Ops:
  0.6 1.0 copy.47
  1.9 1.2 reduce-window.6
  3.7 2.9 %mul.206 = f32[256,2,1024]{2,1,0:T(2,128)} broadcast(bf16[256,1024]{1,0:T(8,128)(2,1)} %param.15), dimensions={0,2} | broadcast | bytes 2621440 | tf_op jit(solution)/shard_map/mul | solution.py:242
  6.6 3.7 %mul.207 = f32[512,1024]{1,0:T(8,128)} reshape(f32[256,2,1024]{2,1,0:T(2,128)} %mul.206) | data formatting | bytes 4194304 | tf_op jit(solution)/shard_map/mul | solution.py:242
  11.4 1.8 all-gather.2
  13.2 3.0 %fusion.12 = bf16[1024,1024]{0,1:T(8,128)(2,1)S(1)} fusion(f32[512,1024]{1,0:T(8,128)} %mul.207, f32[512]{0:T(512)S(1)} %mul.204, s32[512]{0:T(512)S(1)} %multiply_add_fusion), kind=kOutput, calls=%fused_computation.33 | convolution fusion | flops 1076363264 | bytes 4198400 | tf_op jit(solution)/shard_map/dot_general | solution.py:201
  16.2 0.8 convolution_convert_fusion.1
  17.0 2.5 %pad_maximum_fusion = bf16[1024,2048]{0,1:T(8,128)(2,1)} fusion(bf16[1024,1024]{0,1:T(8,128)(2,1)S(1)} %fusion.12, bf16[1024,1024]{0,1:T(8,128)(2,1)S(1)} %convolution_convert_fusion.1), kind=kLoop, calls=%fused_computation.2 | loop fusion | flops 8388608 | bytes 8388608 | tf_op jit(solution)/shard_map/concatenate | solution.py:248
  19.5 6.4 %copy.52 = bf16[1024,2048]{1,0:T(8,128)(2,1)} copy(bf16[1024,2048]{0,1:T(8,128)(2,1)} %pad_maximum_fusion) | data formatting | bytes 8388608 | tf_op jit(solution)/shard_map/concatenate | solution.py:248
  25.9 2.2 copy-done.2
  28.1 61.2 %dispatch.1 = bf16[2,64,16,2048]{3,2,1,0:T(8,128)(2,1)S(1)} custom-call(bf16[64,16,2048]{2,1,0:T(8,128)(2,1)S(1)} %bitcast.84), custom_call_target="tpu_custom_call" | custom-call | tf_op jit(solution)/shard_map/dispatch/pallas_call | solution.py:105
  89.4 1.0 slice_bitcast_fusion.3
  90.9 2.3 %fusion.6 = f32[1024,512]{1,0:T(8,128)S(1)} fusion(bf16[1,2048,512]{2,1,0:T(8,128)(2,1)S(1)} %copy-done.19, bf16[1024,1024]{1,0:T(8,128)(2,1)S(1)} %get-tuple-element.13, bf16[1024,1024]{1,0:T(8,128)(2,1)S(1)} %get-tuple-element.14), kind=kOutput, calls=%fused_computation.20 | convolution fusion | flops 2155872256 | bytes 8388608 | tf_op jit(solution)/shard_map/dot_general | solution.py:257
  93.3 2.3 %fusion.3 = f32[1024,512]{1,0:T(8,128)S(1)} fusion(bf16[1,2048,512]{2,1,0:T(8,128)(2,1)S(1)} %copy-done, bf16[1024,1024]{1,0:T(8,128)(2,1)S(1)} %get-tuple-element.13, bf16[1024,1024]{1,0:T(8,128)(2,1)S(1)} %get-tuple-element.14), kind=kOutput, calls=%fused_computation.17 | convolution fusion | flops 2155872256 | bytes 8388608 | tf_op jit(solution)/shard_map/dot_general | solution.py:256
  95.7 3.2 %multiply_convert_fusion.1 = (bf16[1024,512]{1,0:T(8,128)(2,1)S(1)}, bf16[1024,512]{1,0:T(8,128)(2,1)S(1)}) fusion(f32[1024,512]{1,0:T(8,128)S(1)} %fusion.3, f32[1024,512]{1,0:T(8,128)S(1)} %fusion.6, bf16[1,512,2048]{2,1,0:T(8,128)(2,1)S(1)} %copy-done.18, bf16[1024,1024]{1,0:T(8,128)(2,1)S(1)} %get-tuple-element.15, ...), kind=kOutput, calls=%fused_computation.24 | convolution fusion | flops 2162688000 | bytes 12582912 | tf_op jit(solution)/shard_map/dot_general | solution.py:211
  98.9 2.4 %fusion.1 = f32[1024,2048]{1,0:T(8,128)S(1)} fusion(bf16[1024,512]{1,0:T(8,128)(2,1)S(1)} %get-tuple-element.17, bf16[1,2048,512]{2,1,0:T(8,128)(2,1)S(1)} %copy-done), kind=kOutput, calls=%fused_computation.15 | convolution fusion | flops 2147483648 | bytes 11534336 | tf_op jit(solution)/shard_map/dot_general | solution.py:211
  101.3 2.4 %add_convert_fusion = bf16[1024,2048]{1,0:T(8,128)(2,1)S(1)} fusion(f32[1024,2048]{1,0:T(8,128)S(1)} %fusion.1, bf16[1024,512]{1,0:T(8,128)(2,1)S(1)} %get-tuple-element.16, bf16[1,2048,512]{2,1,0:T(8,128)(2,1)S(1)} %copy-done.19), kind=kOutput, calls=%fused_computation | convolution fusion | flops 2151677952 | bytes 15728640 | tf_op jit(solution)/shard_map/dot_general | solution.py:211
  104.1 8.2 %all_to_all.10 = bf16[2,1024,1024]{2,1,0:T(8,128)(2,1)} all-to-all(bf16[2,1024,1024]{2,1,0:T(8,128)(2,1)S(1)} %bitcast.88), channel_id=1, replica_groups=mesh['sp'=64,'tp'=2] {'tp'}, dimensions={0} | all-to-all | bytes 8388608 | tf_op jit(solution)/shard_map/all_to_all | solution.py:174
  112.3 4.1 %reduce_sum.85 = bf16[1024,1024]{1,0:T(8,128)(2,1)S(1)} reduce(bf16[2,1024,1024]{2,1,0:T(8,128)(2,1)} %all_to_all.10, bf16[]{:T(256)} %constant.20.clone.1), dimensions={0}, to_apply=%region_6.7 | reduce | flops 1048576 | bytes 6291458 | tf_op jit(solution)/shard_map/reduce_sum | solution.py:175
  116.5 32.0 %give_back.1 = bf16[64,16,1024]{2,1,0:T(8,128)(2,1)S(1)} custom-call(bf16[64,16,1024]{2,1,0:T(8,128)(2,1)S(1)} %bitcast.85), custom_call_target="tpu_custom_call" | custom-call | tf_op jit(solution)/shard_map/give_back/pallas_call | solution.py:149
  149.3 1.8 all-gather.3
  151.6 1.1 broadcast_in_dim.8
  152.7 3.6 %all-to-all-start.1 = ((bf16[2,256,1024]{2,1,0:T(8,128)(2,1)}), bf16[2,256,1024]{2,1,0:T(8,128)(2,1)S(1)}, u32[]{:S(2)}, u32[]{:S(2)}) async-start(bf16[2,256,1024]{2,1,0:T(8,128)(2,1)} %broadcast_in_dim.8), calls=%async_computation.1 | async-start | bytes 2097152 | tf_op jit(solution)/shard_map/all_to_all | solution.py:180
  156.4 2.7 %collective-permute-start = (bf16[2,2,512]{2,1,0:T(2,128)(2,1)S(1)}, bf16[2,2,512]{2,1,0:T(2,128)(2,1)S(1)}, u32[]{:S(2)}, u32[]{:S(2)}) collective-permute-start(bf16[2,2,512]{2,1,0:T(2,128)(2,1)S(1)} %pad_maximum_fusion.10), channel_id=1, source_target_pairs={{0,2},{2,4},{4,6},{6,8},{8,10},{10,12},{12,14},{14,16},{16,18},{18... | collective-permute-start | bytes 12296 | tf_op jit(solution)/shard_map/ppermute | solution.py:187
  159.1 7.9 %convolution_bitcast_fusion = f32[1,512,2048]{2,1,0:T(8,128)} fusion(bf16[1024,1024]{1,0:T(8,128)(2,1)} %copy-done.11, bf16[1024,1024]{1,0:T(8,128)(2,1)} %copy-done.10, f32[1024,512]{1,0:T(8,128)} %copy-done.26, f32[1024,512]{1,0:T(8,128)} %copy-done.27), kind=kOutput, calls=%fused_computation.6 | convolution fusion | flops 2159017984 | bytes 12582912 | tf_op jit(solution)/shard_map/dot_general | solution.py:205
  167.0 4.5 %convolution_bitcast_fusion.1 = f32[1,2048,512]{2,1,0:T(8,128)} fusion(bf16[1024,512]{1,0:T(8,128)(2,1)S(1)} %copy-done.23, bf16[1024,1024]{1,0:T(8,128)(2,1)S(1)} %copy-done.7, bf16[1024,1024]{1,0:T(8,128)(2,1)S(1)} %copy-done.9), kind=kOutput, calls=%fused_computation.7 | convolution fusion | flops 2155872256 | bytes 9437184 | tf_op jit(solution)/shard_map/dot_general | solution.py:205
  171.5 4.5 %convolution_bitcast_fusion.2 = f32[1,2048,512]{2,1,0:T(8,128)} fusion(bf16[1024,512]{1,0:T(8,128)(2,1)S(1)} %copy-done.25, bf16[1024,1024]{1,0:T(8,128)(2,1)S(1)} %copy-done.7, bf16[1024,1024]{1,0:T(8,128)(2,1)S(1)} %copy-done.9), kind=kOutput, calls=%fused_computation.8 | convolution fusion | flops 2155872256 | bytes 9437184 | tf_op jit(solution)/shard_map/dot_general | solution.py:205
  177.7 1.5 multiply_convert_fusion.6
  179.2 1.5 collective-permute-start.1
  181.6 35.7 %share.1 = bf16[64,32,512]{2,1,0:T(8,128)(2,1)S(1)} custom-call(bf16[64,32,512]{2,1,0:T(8,128)(2,1)S(1)} %bitcast.87), custom_call_target="tpu_custom_call" | custom-call | tf_op jit(solution)/shard_map/share/pallas_call | solution.py:149
  217.3 0.9 convert_reduce_fusion
  218.2 0.9 fusion.38
  (88 shorter events, 7.6 us)
Async XLA Ops:
  0.6 92.7 %copy-start = (bf16[1,2048,512]{2,1,0:T(8,128)(2,1)S(1)}, bf16[1,2048,512]{2,1,0:T(8,128)(2,1)}, u32[]{:S(2)}) copy-start(bf16[1,2048,512]{2,1,0:T(8,128)(2,1)} %param.23) | copy-start | bytes 6291460
  6.6 3.7 %copy-start.17 = (f32[256,2]{0,1:T(2,128)S(1)}, f32[256,2]{0,1:T(2,128)}, u32[]{:S(2)}) copy-start(f32[256,2]{0,1:T(2,128)} %param.16) | copy-start | bytes 6148
  6.6 4.1 %copy-start.15 = (s32[256,2]{0,1:T(2,128)S(1)}, s32[256,2]{0,1:T(2,128)}, u32[]{:S(2)}) copy-start(s32[256,2]{0,1:T(2,128)} %param.17) | copy-start | bytes 6148
  6.6 4.6 %copy-start.3 = (bf16[256,1024]{1,0:T(8,128)(2,1)S(1)}, bf16[256,1024]{1,0:T(8,128)(2,1)}, u32[]{:S(2)}) copy-start(bf16[256,1024]{1,0:T(8,128)(2,1)} %param.13) | copy-start | bytes 1572868
  13.2 3.0 %copy-start.14 = (f32[1024]{0:T(1024)S(1)}, f32[1024]{0:T(1024)}, u32[]{:S(2)}) copy-start(f32[1024]{0:T(1024)} %param.14) | copy-start | bytes 12292
  25.9 2.2 copy-start.2
  89.3 1.6 copy-start.19
  90.3 2.9 %copy-start.6 = (bf16[1024,1024]{1,0:T(8,128)(2,1)}, bf16[1024,1024]{1,0:T(8,128)(2,1)S(1)}, u32[]{:S(2)}) copy-start(bf16[1024,1024]{1,0:T(8,128)(2,1)S(1)} %get-tuple-element.13) | copy-start | bytes 6291460
  90.3 2.9 %copy-start.8 = (bf16[1024,1024]{1,0:T(8,128)(2,1)}, bf16[1024,1024]{1,0:T(8,128)(2,1)S(1)}, u32[]{:S(2)}) copy-start(bf16[1024,1024]{1,0:T(8,128)(2,1)S(1)} %get-tuple-element.14) | copy-start | bytes 6291460
  90.3 5.3 %copy-start.10 = (bf16[1024,1024]{1,0:T(8,128)(2,1)}, bf16[1024,1024]{1,0:T(8,128)(2,1)S(1)}, u32[]{:S(2)}) copy-start(bf16[1024,1024]{1,0:T(8,128)(2,1)S(1)} %get-tuple-element.12) | copy-start | bytes 6291460
  90.4 5.3 %copy-start.11 = (bf16[1024,1024]{1,0:T(8,128)(2,1)}, bf16[1024,1024]{1,0:T(8,128)(2,1)S(1)}, u32[]{:S(2)}) copy-start(bf16[1024,1024]{1,0:T(8,128)(2,1)S(1)} %get-tuple-element.15) | copy-start | bytes 6291460
  93.3 2.4 %copy-start.26 = (f32[1024,512]{1,0:T(8,128)}, f32[1024,512]{1,0:T(8,128)S(1)}, u32[]{:S(2)}) copy-start(f32[1024,512]{1,0:T(8,128)S(1)} %fusion.6) | copy-start | bytes 6291460
  93.3 2.4 %copy-start.18 = (bf16[1,512,2048]{2,1,0:T(8,128)(2,1)S(1)}, bf16[1,512,2048]{2,1,0:T(8,128)(2,1)}, u32[]{:S(2)}) copy-start(bf16[1,512,2048]{2,1,0:T(8,128)(2,1)} %param.25) | copy-start | bytes 6291460
  95.6 3.2 %copy-start.27 = (f32[1024,512]{1,0:T(8,128)}, f32[1024,512]{1,0:T(8,128)S(1)}, u32[]{:S(2)}) copy-start(f32[1024,512]{1,0:T(8,128)S(1)} %fusion.3) | copy-start | bytes 6291460
  98.9 2.4 %copy-start.24 = (bf16[1024,512]{1,0:T(8,128)(2,1)}, bf16[1024,512]{1,0:T(8,128)(2,1)S(1)}, u32[]{:S(2)}) copy-start(bf16[1024,512]{1,0:T(8,128)(2,1)S(1)} %get-tuple-element.17) | copy-start | bytes 3145732
  98.9 2.4 %copy-start.22 = (bf16[1024,512]{1,0:T(8,128)(2,1)}, bf16[1024,512]{1,0:T(8,128)(2,1)S(1)}, u32[]{:S(2)}) copy-start(bf16[1024,512]{1,0:T(8,128)(2,1)S(1)} %get-tuple-element.16) | copy-start | bytes 3145732
  148.4 2.7 %copy-start.4 = (bf16[256,1024]{1,0:T(8,128)(2,1)S(1)}, bf16[256,1024]{1,0:T(8,128)(2,1)}, u32[]{:S(2)}) copy-start(bf16[256,1024]{1,0:T(8,128)(2,1)} %param.15) | copy-start | bytes 1572868
  151.6 15.4 %copy-start.5 = (bf16[256,1024]{1,0:T(8,128)(2,1)}, bf16[256,1024]{1,0:T(8,128)(2,1)S(1)}, u32[]{:S(2)}) copy-start(bf16[256,1024]{1,0:T(8,128)(2,1)S(1)} %fusion.20) | copy-start | bytes 1572868
  151.6 4.7 %copy-start.12 = (bf16[256,512]{1,0:T(8,128)(2,1)S(1)}, bf16[256,512]{1,0:T(8,128)(2,1)}, u32[]{:S(2)}) copy-start(bf16[256,512]{1,0:T(8,128)(2,1)} %param.18) | copy-start | bytes 786436
  151.6 4.7 %copy-start.13 = (bf16[256,512]{1,0:T(8,128)(2,1)S(1)}, bf16[256,512]{1,0:T(8,128)(2,1)}, u32[]{:S(2)}) copy-start(bf16[256,512]{1,0:T(8,128)(2,1)} %param.20) | copy-start | bytes 786436
  152.7 23.4 %all-to-all-start.1 = ((bf16[2,256,1024]{2,1,0:T(8,128)(2,1)}), bf16[2,256,1024]{2,1,0:T(8,128)(2,1)S(1)}, u32[]{:S(2)}, u32[]{:S(2)}) async-start(bf16[2,256,1024]{2,1,0:T(8,128)(2,1)} %broadcast_in_dim.8), calls=%async_computation.1 | async-start | bytes 2097152 | tf_op jit(solution)/shard_map/all_to_all | solution.py:180
  156.3 10.7 %copy-start.7 = (bf16[1024,1024]{1,0:T(8,128)(2,1)S(1)}, bf16[1024,1024]{1,0:T(8,128)(2,1)}, u32[]{:S(2)}) copy-start(bf16[1024,1024]{1,0:T(8,128)(2,1)} %copy-done.6) | copy-start | bytes 6291460
  156.4 10.7 %copy-start.9 = (bf16[1024,1024]{1,0:T(8,128)(2,1)S(1)}, bf16[1024,1024]{1,0:T(8,128)(2,1)}, u32[]{:S(2)}) copy-start(bf16[1024,1024]{1,0:T(8,128)(2,1)} %copy-done.8) | copy-start | bytes 6291460
  156.4 10.6 %copy-start.23 = (bf16[1024,512]{1,0:T(8,128)(2,1)S(1)}, bf16[1024,512]{1,0:T(8,128)(2,1)}, u32[]{:S(2)}) copy-start(bf16[1024,512]{1,0:T(8,128)(2,1)} %copy-done.22) | copy-start | bytes 3145732
  156.4 20.3 %collective-permute-start = (bf16[2,2,512]{2,1,0:T(2,128)(2,1)S(1)}, bf16[2,2,512]{2,1,0:T(2,128)(2,1)S(1)}, u32[]{:S(2)}, u32[]{:S(2)}) collective-permute-start(bf16[2,2,512]{2,1,0:T(2,128)(2,1)S(1)} %pad_maximum_fusion.10), channel_id=1, source_target_pairs={{0,2},{2,4},{4,6},{6,8},{8,10},{10,12},{12,14},{14,16},{16,18},{18... | collective-permute-start | bytes 12296 | tf_op jit(solution)/shard_map/ppermute | solution.py:187
  167.0 4.5 %copy-start.25 = (bf16[1024,512]{1,0:T(8,128)(2,1)S(1)}, bf16[1024,512]{1,0:T(8,128)(2,1)}, u32[]{:S(2)}) copy-start(bf16[1024,512]{1,0:T(8,128)(2,1)} %copy-done.24) | copy-start | bytes 3145732
  176.0 0.7 copy-start.16
  176.0 1.0 copy-start.21
  176.1 1.6 copy-start.20
  179.2 39.0 %collective-permute-start.1 = (f32[2,512]{1,0:T(2,128)S(1)}, f32[2,512]{1,0:T(2,128)S(1)}, u32[]{:S(2)}, u32[]{:S(2)}) collective-permute-start(f32[2,512]{1,0:T(2,128)S(1)} %slice.94), channel_id=1, source_target_pairs={{2,0},{4,2},{6,4},{8,6},{10,8},{12,10},{14,12},{16,14},{18,16},{20... | collective-permute-start | bytes 12296 | tf_op jit(solution)/shard_map/ppermute | solution.py:187
  181.6 38.4 %copy-start.1 = (bf16[1,2048,512]{2,1,0:T(8,128)(2,1)S(1)}, bf16[1,2048,512]{2,1,0:T(8,128)(2,1)}, u32[]{:S(2)}) copy-start(bf16[1,2048,512]{2,1,0:T(8,128)(2,1)} %param.23) | copy-start | bytes 6291460

commit v2 on v0

v2 whole, which is shorter than its diff:
```python
import functools

import jax
import jax.numpy as jnp
from jax import lax
from jax.experimental import pallas as pl
from jax.experimental.pallas import tpu as pltpu
from jax.sharding import PartitionSpec as P

D = 2048
EPSILON = 1e-06
MESH = pl.DeviceIdType.MESH
SIDE = 4
CHIPS = SIDE**3


def _parts(k):
    return k // 16, (k // 4) % 4, k % 4


def _join(z, y, x):
    return (z % 4) * 16 + (y % 4) * 4 + x % 4


def _shift_order():
    hops = lambda k: sum(min(a, SIDE - a) for a in _parts(k))
    turn = lambda k: _join(*(_parts(k)[1:] + _parts(k)[:1]))
    back = lambda k: _join(*(-a for a in _parts(k)))
    order = []
    for k in sorted(range(1, CHIPS), key=lambda k: -hops(k)):
        for kk in (k, turn(k), turn(turn(k))):
            for other in (kk,):
                if other not in order:
                    order.append(other)
        for kk in (k, turn(k), turn(turn(k))):
            if back(kk) not in order:
                order.append(back(kk))
    return order


ORDER = _shift_order()


def moved(me, k, sign=1):
    z, y, x = me // 16, lax.rem(me // 4, 4), lax.rem(me, 4)
    kz, ky, kx = (a if sign > 0 else (SIDE - a) % SIDE for a in _parts(k))
    return lax.rem(z + kz, 4) * 16 + lax.rem(y + ky, 4) * 4 + lax.rem(x + kx, 4)


GROUPS = 8
BLOCKS = CHIPS // GROUPS


def greet_all(me, core):
    barrier = pltpu.get_barrier_semaphore()
    for k in ORDER:
        pl.semaphore_signal(
            barrier, inc=1, device_id=(moved(me, k), core), device_id_type=MESH
        )
    pl.semaphore_signal(barrier, inc=1, device_id=(me, 1 - core), device_id_type=MESH)
    return barrier


def remote(source, target, send_sem, recv_sem, peer):
    return pltpu.make_async_remote_copy(
        src_ref=source,
        dst_ref=target,
        send_sem=send_sem,
        recv_sem=recv_sem,
        device_id=peer,
        device_id_type=MESH,
    )


def wait_for(ref, sem):
    pltpu.make_async_copy(ref, ref, sem).wait()


def dot(left, right, over=(1, 0)):
    return lax.dot_general(
        left, right, (((over[0],), (over[1],)), ((), ())), preferred_element_type=jnp.float32
    )


def experts_kernel(
    routes,
    weights,
    stream,
    gain,
    cot,
    gate_hbm,
    up_hbm,
    down_hbm,
    normed_grad,
    inverse_out,
    gate_g,
    up_g,
    down_g,
    gate_w,
    up_w,
    down_w,
    square,
    normed,
    select,
    send,
    rows_in,
    pre,
    hid,
    theirs,
    mine,
    other,
    ret,
    back,
    load_sem,
    square_sem,
    send_sem,
    recv_sem,
    pass_send,
    pass_recv,
    part_send,
    part_recv,
    back_send,
    back_recv,
):
    me, core = lax.axis_index("sp"), lax.axis_index("tp")
    partner = (me, 1 - core)
    capacity = send.shape[0] // CHIPS
    half = stream.shape[1]
    depth = BLOCKS * capacity
    width = gate_w.shape[1]
    barrier = greet_all(me, core)
    loads = [
        pltpu.make_async_copy(a, b, load_sem.at[i])
        for i, (a, b) in enumerate(((gate_hbm, gate_w), (up_hbm, up_w), (down_hbm, down_w)))
    ]
    for load in loads:
        load.start()
    stream_float = stream[...].astype(jnp.float32)
    part = jnp.sum(stream_float * stream_float, axis=1, keepdims=True)
    square[0] = jnp.broadcast_to(part, square.shape[1:])
    pl.semaphore_wait(barrier, CHIPS)
    swap = remote(square.at[0], square.at[1], square_sem.at[0], square_sem.at[1], partner)
    swap.start()

    tokens = stream.shape[0]
    first, second = routes[0:1, :], routes[1:2, :]
    expert = lax.broadcasted_iota(jnp.int32, (CHIPS, tokens), 0)
    on_first, on_second = expert == first, expert == second
    named = jnp.where(on_first | on_second, 1.0, 0.0).astype(jnp.bfloat16)
    before = lax.broadcasted_iota(jnp.int32, (tokens, tokens), 0) < lax.broadcasted_iota(
        jnp.int32, (tokens, tokens), 1
    )
    earlier = dot(named, jnp.where(before, 1.0, 0.0).astype(jnp.bfloat16))

    def target_of(on, route):
        rank = jnp.sum(jnp.where(on, earlier, 0.0), axis=0, keepdims=True)
        return route * capacity + rank.astype(jnp.int32)

    first_target, second_target = target_of(on_first, first), target_of(on_second, second)
    chunk = 256
    slot_weights = []
    for at in range(0, CHIPS * capacity, chunk):
        place = lax.broadcasted_iota(jnp.int32, (chunk, tokens), 0) + at
        is_first, is_second = place == first_target, place == second_target
        select[at : at + chunk] = jnp.where(is_first | is_second, 1.0, 0.0).astype(jnp.bfloat16)
        slot_weights.append(
            jnp.sum(
                jnp.where(is_first, weights[0:1, :], 0.0)
                + jnp.where(is_second, weights[1:2, :], 0.0),
                axis=1,
                keepdims=True,
            )
        )
    swap.wait()
    inverse = lax.rsqrt((square[0, :, 0:1] + square[1, :, 0:1]) / D + EPSILON)
    inverse_out[...] = jnp.broadcast_to(inverse, inverse_out.shape)
    normed[...] = (stream_float * inverse * gain[...]).astype(jnp.bfloat16)
    for i, at in enumerate(range(0, CHIPS * capacity, chunk)):
        chosen = select[at : at + chunk]
        send[at : at + chunk, :half] = dot(chosen, normed[...]).astype(jnp.bfloat16)
        send[at : at + chunk, half:] = (slot_weights[i] * dot(chosen, cot[...])).astype(
            jnp.bfloat16
        )

    def block(index):
        return pl.ds(pl.multiple_of(index * capacity, capacity), capacity)

    for j, k in enumerate(ORDER):
        peer = moved(me, k)
        remote(
            send.at[block(peer)],
            rows_in.at[core, pl.ds(j * capacity, capacity)],
            send_sem,
            recv_sem.at[j // BLOCKS],
            (peer, core),
        ).start()
    rows_in[core, (CHIPS - 1) * capacity :] = send[block(me)]
    for load in loads:
        load.wait()

    def group(g, count=depth):
        return pl.ds(pl.multiple_of(g * depth, depth), count)

    def passing(g):
        piece = rows_in.at[core, group(g)]
        return remote(piece, piece, pass_send.at[g], pass_recv.at[g], partner)

    def exchange(g):
        return remote(
            theirs.at[group(g)], other.at[group(g)], part_send.at[g], part_recv.at[g], partner
        )

    def take(g):
        @pl.when(g < GROUPS - 1)
        def _():
            wait_for(rows_in.at[core, group(g)], recv_sem.at[g])

        @pl.when(g == GROUPS - 1)
        def _():
            wait_for(rows_in.at[core, group(g, depth - capacity)], recv_sem.at[g])

        passing(g).start()

    def compute(g):
        wait_for(rows_in.at[1 - core, group(g)], pass_recv.at[g])
        rows = group(g)
        gate_lin = dot(rows_in[0, rows, :half], gate_w[:half]) + dot(
            rows_in[1, rows, :half], gate_w[half:]
        )
        up_lin = dot(rows_in[0, rows, :half], up_w[:half]) + dot(
            rows_in[1, rows, :half], up_w[half:]
        )
        hidden_grad = dot(rows_in[0, rows, half:], down_w[:, :half], (1, 1)) + dot(
            rows_in[1, rows, half:], down_w[:, half:], (1, 1)
        )
        sigmoid_gate = jax.nn.sigmoid(gate_lin)
        silu_gate = gate_lin * sigmoid_gate
        hid[rows] = (silu_gate * up_lin).astype(jnp.bfloat16)
        gate_pre = (
            hidden_grad * up_lin * sigmoid_gate * (1.0 + gate_lin * (1.0 - sigmoid_gate))
        ).astype(jnp.bfloat16)
        up_pre = (hidden_grad * silu_gate).astype(jnp.bfloat16)
        pre[rows, :width] = gate_pre
        pre[rows, width:] = up_pre
        for target, side in ((theirs, 1 - core), (mine, core)):
            features = pl.ds(pl.multiple_of(side * half, half), half)
            value = dot(gate_pre, gate_w[features], (1, 1)) + dot(up_pre, up_w[features], (1, 1))
            target[rows] = value.astype(jnp.bfloat16)
        exchange(g).start()

    def finish(g):
        wait_for(other.at[group(g)], part_recv.at[g])
        rows = group(g)
        ret[rows] = (mine[rows].astype(jnp.float32) + other[rows].astype(jnp.float32)).astype(
            jnp.bfloat16
        )
        for i in range(BLOCKS):
            k = jnp.int32(ORDER[i])
            for later in range(1, GROUPS):
                if later * BLOCKS + i < CHIPS - 1:
                    k = jnp.where(g == later, ORDER[later * BLOCKS + i], k)
            z = lax.rem(me // 16 + 4 - k // 16, 4)
            y = lax.rem(lax.rem(me // 4, 4) + 4 - lax.rem(k // 4, 4), 4)
            x = lax.rem(lax.rem(me, 4) + 4 - lax.rem(k, 4), 4)
            go = remote(
                ret.at[block(g * BLOCKS + i)],
                back.at[block(me)],
                back_send,
                back_recv,
                (z * 16 + y * 4 + x, core),
            )
            if i < BLOCKS - 1:
                go.start()
            else:
                pl.when(g < GROUPS - 1)(go.start)

    def step(i, carry):
        pl.when(i < GROUPS)(lambda: take(i))
        pl.when((i >= 1) & (i <= GROUPS))(lambda: compute(i - 1))
        pl.when(i >= 2)(lambda: finish(i - 2))
        return carry

    lax.fori_loop(0, GROUPS + 2, step, 0)
    back[block(me)] = ret[(CHIPS - 1) * capacity :]

    tile = 256

    def gate_step(i, carry):
        side, at = i // (half // tile), lax.rem(i, half // tile)
        columns = pl.ds(pl.multiple_of(at * tile, tile), tile)
        value = dot(rows_in[side, :, columns], pre[...], (0, 0))
        features = pl.ds(pl.multiple_of(i * tile, tile), tile)
        gate_g[features] = value[:, :width]
        up_g[features] = value[:, width:]
        return carry

    lax.fori_loop(0, D // tile, gate_step, 0)

    def down_step(i, carry):
        side, at = i // 2, lax.rem(i, 2)
        columns = pl.ds(pl.multiple_of(half + at * 512, 512), 512)
        down_g[:, pl.ds(pl.multiple_of(i * 512, 512), 512)] = dot(
            hid[...], rows_in[side, :, columns], (0, 0)
        )
        return carry

    lax.fori_loop(0, 4, down_step, 0)
    sent = (CHIPS - 1) * capacity
    wait_for(back.at[pl.ds(0, sent)], back_recv)
    normed_grad[...] = dot(select[...], back[...], (0, 0))
    wait_for(send.at[pl.ds(0, sent)], send_sem)
    wait_for(ret.at[pl.ds(0, sent)], back_send)
    for g in range(GROUPS):
        passing(g).wait_send()
        exchange(g).wait_send()


def experts(routes, weights, stream, gain, cot, gate_w, up_w, down_w):
    tokens, half = stream.shape
    slots = 2 * tokens * routes.shape[0]
    width = gate_w.shape[1]
    vmem = pl.BlockSpec(memory_space=pltpu.VMEM)
    hbm = pl.BlockSpec(memory_space=pl.ANY)
    f32, bf16 = jnp.float32, jnp.bfloat16
    dma = pltpu.SemaphoreType.DMA
    return pl.pallas_call(
        experts_kernel,
        out_shape=(
            jax.ShapeDtypeStruct((tokens, half), f32),
            jax.ShapeDtypeStruct((tokens, 128), f32),
            jax.ShapeDtypeStruct((D, width), f32),
            jax.ShapeDtypeStruct((D, width), f32),
            jax.ShapeDtypeStruct((width, D), f32),
        ),
        in_specs=[vmem] * 5 + [hbm] * 3,
        out_specs=(vmem,) * 5,
        scratch_shapes=[
            pltpu.VMEM((D, width), bf16),
            pltpu.VMEM((D, width), bf16),
            pltpu.VMEM((width, D), bf16),
            pltpu.VMEM((2, tokens, 128), f32),
            pltpu.VMEM((tokens, half), bf16),
            pltpu.VMEM((slots, tokens), bf16),
            pltpu.VMEM((slots, 2 * half), bf16),
            pltpu.VMEM((2, slots, 2 * half), bf16),
            pltpu.VMEM((slots, 2 * width), bf16),
            pltpu.VMEM((slots, width), bf16),
            pltpu.VMEM((slots, half), bf16),
            pltpu.VMEM((slots, half), bf16),
            pltpu.VMEM((slots, half), bf16),
            pltpu.VMEM((slots, half), bf16),
            pltpu.VMEM((slots, half), bf16),
            dma((3,)),
            dma((2,)),
            dma(()),
            dma((GROUPS,)),
            dma((GROUPS,)),
            dma((GROUPS,)),
            dma((GROUPS,)),
            dma((GROUPS,)),
            dma(()),
            dma(()),
        ],
        compiler_params=pltpu.CompilerParams(
            collective_id=0, has_side_effects=True, vmem_limit_bytes=60 << 20
        ),
        name="experts",
    )(routes, weights, stream, gain, cot, gate_w, up_w, down_w)


def tail_kernel(
    normed_grad,
    inverse_in,
    stream,
    gain,
    cot,
    value_in,
    out_gate,
    in_gate,
    taps,
    out_proj,
    stream_grad,
    proj_grad,
    input_grad,
    bgate_grad,
    cgate_grad,
    cross,
    whole,
    rim_in,
    rim_out,
    rim_back,
    conv,
    delta,
    shares,
    arrived,
    cross_sem,
    whole_sem,
    rim_sem,
    back_sem,
    share_sem,
):
    me, core = lax.axis_index("sp"), lax.axis_index("tp")
    partner = (me, 1 - core)
    tokens, half = stream.shape
    barrier = greet_all(me, core)
    stream_float = stream[...].astype(jnp.float32)
    part = jnp.sum(stream_float * gain[...] * normed_grad[...], axis=1, keepdims=True)
    cross[0] = jnp.broadcast_to(part, cross.shape[1:])
    pl.semaphore_wait(barrier, CHIPS)
    swap = remote(cross.at[0], cross.at[1], cross_sem.at[0], cross_sem.at[1], partner)
    swap.start()
    after, ahead = lax.rem(me + 1, CHIPS), lax.rem(me + CHIPS - 1, CHIPS)
    rims = [
        remote(
            ref.at[pl.ds(tokens - 16, 16)],
            rim_in.at[i],
            rim_sem.at[i],
            rim_sem.at[2 + i],
            (after, core),
        )
        for i, ref in enumerate((value_in, in_gate))
    ]
    for rim in rims:
        rim.start()
    swap.wait()
    inverse = inverse_in[:, 0:1]
    total = cross[0, :, 0:1] + cross[1, :, 0:1]
    grad = (
        cot[...].astype(jnp.float32)
        + inverse * gain[...] * normed_grad[...]
        - stream_float * inverse * inverse * inverse * total / D
    ).astype(jnp.bfloat16)
    stream_grad[...] = grad
    whole[core] = grad
    join = remote(
        whole.at[core], whole.at[core], whole_sem.at[0], whole_sem.at[1], partner
    )
    join.start()

    row = lax.broadcasted_iota(jnp.int32, conv.shape, 0)
    gated = in_gate[...].astype(jnp.float32) * value_in[...].astype(jnp.float32)
    for rim in rims:
        rim.wait()
    rim_gated = rim_in[1].astype(jnp.float32) * rim_in[0].astype(jnp.float32)
    rim_gated = jnp.where(me == 0, jnp.zeros_like(rim_gated), rim_gated)
    last, older = rim_gated[15:16], rim_gated[14:15]
    previous = jnp.where(row == 0, last, pltpu.roll(gated, 1, 0))
    before = jnp.where(row == 0, older, jnp.where(row == 1, last, pltpu.roll(gated, 2, 0)))
    conv[...] = taps[0:1] * before + taps[1:2] * previous + taps[2:3] * gated
    mixer_out = (out_gate[...].astype(jnp.float32) * conv[...]).astype(jnp.bfloat16)
    wait_for(whole.at[1 - core], whole_sem.at[1])
    mixer_grad = dot(whole[0], out_proj[:half]) + dot(whole[1], out_proj[half:])
    delta[...] = mixer_grad * out_gate[...].astype(jnp.float32)
    rim_out[...] = delta[0:8]
    give = remote(rim_out, rim_back, back_sem.at[0], back_sem.at[1], (ahead, core))
    for side in range(2):
        shares[side * half : (side + 1) * half] = dot(whole[side], mixer_out, (0, 0)).astype(
            jnp.bfloat16
        )
    give.start()
    height = proj_grad.shape[0]
    for j, k in enumerate(ORDER):
        peer = moved(me, k)
        remote(
            shares.at[pl.ds(pl.multiple_of(peer * height, height), height)],
            arrived.at[j],
            share_sem.at[0],
            share_sem.at[1],
            (peer, core),
        ).start()
    arrived[CHIPS - 1] = shares[pl.ds(pl.multiple_of(me * height, height), height)]
    bgate_grad[...] = (mixer_grad * conv[...]).astype(jnp.bfloat16)
    give.wait()
    rim_delta = jnp.where(me == CHIPS - 1, jnp.zeros_like(rim_back[...]), rim_back[...])
    nearest, second = rim_delta[0:1], rim_delta[1:2]
    here = delta[...]
    following = jnp.where(row == tokens - 1, nearest, pltpu.roll(here, tokens - 1, 0))
    beyond = jnp.where(
        row == tokens - 2,
        nearest,
        jnp.where(row == tokens - 1, second, pltpu.roll(here, tokens - 2, 0)),
    )
    gated_grad = taps[2:3] * here + taps[1:2] * following + taps[0:1] * beyond
    input_grad[...] = (gated_grad * in_gate[...].astype(jnp.float32)).astype(jnp.bfloat16)
    cgate_grad[...] = (gated_grad * value_in[...].astype(jnp.float32)).astype(jnp.bfloat16)
    wait_for(arrived.at[pl.ds(0, CHIPS - 1)], share_sem.at[1])
    total = arrived[0].astype(jnp.float32)
    for j in range(1, CHIPS):
        total = total + arrived[j].astype(jnp.float32)
    proj_grad[...] = total
    wait_for(shares.at[pl.ds(0, (CHIPS - 1) * height)], share_sem.at[0])
    wait_for(whole.at[core], whole_sem.at[0])


def tail(normed_grad, inverse, stream, gain, cot, value_in, out_gate, in_gate, taps, out_proj):
    tokens, half = stream.shape
    width = value_in.shape[1]
    height = D // CHIPS
    vmem = pl.BlockSpec(memory_space=pltpu.VMEM)
    f32, bf16 = jnp.float32, jnp.bfloat16
    dma = pltpu.SemaphoreType.DMA
    return pl.pallas_call(
        tail_kernel,
        out_shape=(
            jax.ShapeDtypeStruct((tokens, half), bf16),
            jax.ShapeDtypeStruct((height, width), f32),
            jax.ShapeDtypeStruct((tokens, width), bf16),
            jax.ShapeDtypeStruct((tokens, width), bf16),
            jax.ShapeDtypeStruct((tokens, width), bf16),
        ),
        in_specs=[vmem] * 10,
        out_specs=(vmem,) * 5,
        scratch_shapes=[
            pltpu.VMEM((2, tokens, 128), f32),
            pltpu.VMEM((2, tokens, half), bf16),
            pltpu.VMEM((2, 16, width), bf16),
            pltpu.VMEM((8, width), f32),
            pltpu.VMEM((8, width), f32),
            pltpu.VMEM((tokens, width), f32),
            pltpu.VMEM((tokens, width), f32),
            pltpu.VMEM((D, width), bf16),
            pltpu.VMEM((CHIPS, height, width), bf16),
            dma((2,)),
            dma((2,)),
            dma((4,)),
            dma((2,)),
            dma((2,)),
        ],
        compiler_params=pltpu.CompilerParams(
            collective_id=1, has_side_effects=True, vmem_limit_bytes=24 << 20
        ),
        name="tail",
    )(normed_grad, inverse, stream, gain, cot, value_in, out_gate, in_gate, taps, out_proj)


def local(
    stream,
    norm_gain,
    cotangent,
    route_weights,
    routes,
    conv_input,
    conv_bgate,
    conv_cgate,
    conv_taps,
    out_proj,
    gate_weight,
    up_weight,
    down_weight,
):
    gain = norm_gain[None, :]
    normed_grad, inverse, gate_g, up_g, down_g = experts(
        routes.T,
        route_weights.T,
        stream,
        gain,
        cotangent,
        gate_weight[0],
        up_weight[0],
        down_weight[0],
    )
    stream_grad, proj_grad, input_grad, bgate_grad, cgate_grad = tail(
        normed_grad,
        inverse,
        stream,
        gain,
        cotangent,
        conv_input,
        conv_bgate,
        conv_cgate,
        conv_taps,
        out_proj,
    )
    return (
        stream_grad,
        proj_grad,
        input_grad,
        bgate_grad,
        cgate_grad,
        gate_g[None],
        up_g[None],
        down_g[None],
    )


def solution(mesh):
    return jax.shard_map(
        local,
        mesh=mesh,
        in_specs=(
            P("sp", "tp"),
            P("tp"),
            P("sp", "tp"),
            P("sp", None),
            P("sp", None),
            P("sp", "tp"),
            P("sp", "tp"),
            P("sp", "tp"),
            P(None, "tp"),
            P(None, "tp"),
            P("sp", None, "tp"),
            P("sp", None, "tp"),
            P("sp", "tp", None),
        ),
        out_specs=(
            P("sp", "tp"),
            P("sp", "tp"),
            P("sp", "tp"),
            P("sp", "tp"),
            P("sp", "tp"),
            P("sp", None, "tp"),
            P("sp", None, "tp"),
            P("sp", "tp", None),
        ),
        check_vma=False,
    )
```

time: 305 us -> 150 us (0.49)
  Pallas kernels: 0 us -> 133 us
  waiting for transfers between devices: 113 us -> 0 us
  blocking collectives: 80.9 us -> 0 us
  matrix products: 45.6 us -> 0 us
  other arithmetic: 17.5 us -> 0 us
  starting transfers between devices: 15.7 us -> 0 us
  between operations: 14.2 us -> 0.8 us
    pallas_call x0 -> x2, Pallas kernels: none -> 133 us  [the longest x1 95.5 us: experts(): pl.pallas_call(experts_kernel, out_shape=(jax.ShapeDtypeStruct((tokens, h...]
    all_to_all x3 -> x0, blocking collectives: 77.3 us -> none  [the longest x1 64.4 us: side_by_side(): lax.all_to_all(both, axis, split_axis=split_dim, concat_axis=concat_dim,...]
    reduce_scatter x3 -> x0, waiting for transfers between devices: 69 us -> none  [sum_by_axis(): subtotal = lax.psum_scatter(subtotal, axis, scatter_dimension=0, tiled=True)]
    dot_general x13 -> x0, matrix products: 45.6 us -> none  [the longest x5 24.9 us: contract_rows(): lax.dot_general(left, right, (((0,), (0,)), ((), ())), preferred_element_...]
    all_gather x1 -> x0, waiting for transfers between devices: 19.3 us -> none  [sent_together(): lax.all_gather(both, axis, axis=dim, tiled=True)]
    ppermute x2 -> x0, waiting for transfers between devices: 16.6 us -> none  [shifted(): lax.ppermute(value, axis, [(source, source + steps) for source in range(l...]
    unnamed x48 -> x34, local copies, waits for them, and re-layouts: 1.21 us -> 15.1 us
    all_to_all x1 -> x0, starting transfers between devices: 10.6 us -> none  [local(): lax.all_to_all(row_grads, SP, split_axis=0, concat_axis=0, tiled=True)]
  transfers between devices with their start and end apart: 7 -> 0, of which waited for: 6 -> 0; matrix products, arithmetic and copies ran while one was open for 8% -> 0% of each run, Pallas kernels for 0% -> 0%
where the time goes in v2:
time: 150 us; the launch traced here: 149 us
  Pallas kernels  133 us (89%)
  local copies, waits for them, and re-layouts  15.1 us (10%)
    pallas_call x1, Pallas kernels, experts(): pl.pallas_call(experts_kernel, out_shape=(jax.ShapeDtypeStruct((tokens, h...  95.5 us
    pallas_call x1, Pallas kernels, tail(): pl.pallas_call(tail_kernel, out_shape=(jax.ShapeDtypeStruct((tokens, half...  37.7 us
    unnamed x34, local copies, waits for them, and re-layouts  15.1 us

profile of v2, /device:TPU:0, one launch (start us, length us, event | category | flops | bytes accessed | tf_op | source)
XLA Modules:
  0.0 149.1 jit_solution(4782268099165348836)
XLA Ops:
  0.6 0.0 copy-start.1
  0.6 0.0 copy-start
  0.7 0.0 copy-start.2
  0.7 0.0 copy-start.9
  0.7 0.0 copy-start.6
  0.7 0.0 copy-start.5
  0.7 0.0 copy-start.4
  0.7 0.0 copy-start.8
  0.7 95.5 %experts.1 = (f32[256,1024]{1,0:T(8,128)}, f32[256,128]{1,0:T(8,128)}, f32[2048,512]{1,0:T(8,128)}, f32[2048,512]{1,0:T(8,128)}, f32[512,2048]{1,0:T(8,128)}) custom-call(s32[2,256]{1,0:T(2,128)} %bitcast.17, f32[2,256]{1,0:T(2,128)} %bitcast.18, bf16[256,1024]{1,0:T(8,128)(2,1)} %stream.3, f32[1,1024]{1,0:T(1,128)} %bitcast.9, bf16[256,1024]{1,0:T(8,128)(2,1)} %cot.3, ...), custom_call_target="tpu_custom_call" | custom-call | tf_op jit(solution)/shard_map/experts/pallas_call | solution.py:326
  96.3 0.0 copy-done.1
  96.3 0.0 copy-done
  96.3 0.0 copy-done.2
  96.3 0.0 copy-done.9
  96.3 0.0 copy-done.6
  96.3 0.0 copy-done.5
  96.3 0.0 copy-done.4
  96.3 0.0 copy-done.8
  96.3 0.0 copy-start.3
  96.4 1.2 copy-done.3
  97.6 0.9 copy-done.7
  98.5 37.7 %tail.1 = (bf16[256,1024]{1,0:T(8,128)(2,1)S(1)}, f32[32,512]{1,0:T(8,128)S(1)}, bf16[256,512]{1,0:T(8,128)(2,1)S(1)}, bf16[256,512]{1,0:T(8,128)(2,1)S(1)}, bf16[256,512]{1,0:T(8,128)(2,1)S(1)}) custom-call(f32[256,1024]{1,0:T(8,128)S(1)} %copy-done.3, f32[256,128]{1,0:T(8,128)S(1)} %copy-done.7, bf16[256,1024]{1,0:T(8,128)(2,1)S(1)} %copy-done, ...), custom_call_target="tpu_custom_call" | custom-call | tf_op jit(solution)/shard_map/tail/pallas_call | solution.py:502
  136.2 0.8 copy.29
  136.9 0.6 copy.30
  137.6 0.7 copy.31
  138.3 0.7 copy.32
  139.0 0.7 copy.33
  139.7 0.0 copy-done.12
  139.7 2.1 %copy.34 = f32[1,2048,512]{2,1,0:T(8,128)} copy(f32[1,2048,512]{2,1,0:T(8,128)S(1)} %bitcast.13) | data formatting | bytes 8388608
  141.8 1.6 %copy-done.11 = f32[2048,512]{1,0:T(8,128)S(1)} copy-done((f32[2048,512]{1,0:T(8,128)S(1)}, f32[2048,512]{1,0:T(8,128)}, u32[]{:S(2)}) %copy-start.11) | copy-done | bytes 4194328
  143.4 2.1 %copy.35 = f32[1,2048,512]{2,1,0:T(8,128)} copy(f32[1,2048,512]{2,1,0:T(8,128)S(1)} %bitcast.12) | data formatting | bytes 8388608
  145.5 1.6 %copy-done.10 = f32[512,2048]{1,0:T(8,128)S(1)} copy-done((f32[512,2048]{1,0:T(8,128)S(1)}, f32[512,2048]{1,0:T(8,128)}, u32[]{:S(2)}) %copy-start.10) | copy-done | bytes 4194328
  147.1 2.0 %copy.36 = f32[1,512,2048]{2,1,0:T(8,128)} copy(f32[1,512,2048]{2,1,0:T(8,128)S(1)} %bitcast.11) | data formatting | bytes 8388608
  (4 shorter events, 0.0 us)
Async XLA Ops:
  0.6 95.6 %copy-start.1 = (bf16[256,1024]{1,0:T(8,128)(2,1)S(1)}, bf16[256,1024]{1,0:T(8,128)(2,1)}, u32[]{:S(2)}) copy-start(bf16[256,1024]{1,0:T(8,128)(2,1)} %cot.3) | copy-start | bytes 1572868
  0.6 95.6 %copy-start = (bf16[256,1024]{1,0:T(8,128)(2,1)S(1)}, bf16[256,1024]{1,0:T(8,128)(2,1)}, u32[]{:S(2)}) copy-start(bf16[256,1024]{1,0:T(8,128)(2,1)} %stream.3) | copy-start | bytes 1572868
  0.7 95.6 %copy-start.2 = (bf16[2048,512]{1,0:T(8,128)(2,1)S(1)}, bf16[2048,512]{1,0:T(8,128)(2,1)}, u32[]{:S(2)}) copy-start(bf16[2048,512]{1,0:T(8,128)(2,1)} %out_proj.1) | copy-start | bytes 6291460
  0.7 95.6 %copy-start.9 = (f32[3,512]{1,0:T(4,128)S(1)}, f32[3,512]{1,0:T(4,128)}, u32[]{:S(2)}) copy-start(f32[3,512]{1,0:T(4,128)} %taps.1) | copy-start | bytes 18436
  0.7 95.6 %copy-start.6 = (bf16[256,512]{1,0:T(8,128)(2,1)S(1)}, bf16[256,512]{1,0:T(8,128)(2,1)}, u32[]{:S(2)}) copy-start(bf16[256,512]{1,0:T(8,128)(2,1)} %in_gate.1) | copy-start | bytes 786436
  0.7 95.6 %copy-start.5 = (bf16[256,512]{1,0:T(8,128)(2,1)S(1)}, bf16[256,512]{1,0:T(8,128)(2,1)}, u32[]{:S(2)}) copy-start(bf16[256,512]{1,0:T(8,128)(2,1)} %out_gate.1) | copy-start | bytes 786436
  0.7 95.6 %copy-start.4 = (bf16[256,512]{1,0:T(8,128)(2,1)S(1)}, bf16[256,512]{1,0:T(8,128)(2,1)}, u32[]{:S(2)}) copy-start(bf16[256,512]{1,0:T(8,128)(2,1)} %value_in.1) | copy-start | bytes 786436
  0.7 95.6 %copy-start.8 = (f32[1024]{0:T(1024)S(1)}, f32[1024]{0:T(1024)}, u32[]{:S(2)}) copy-start(f32[1024]{0:T(1024)} %param.14) | copy-start | bytes 12292
  96.3 1.2 copy-start.3
  97.6 0.9 copy-start.7
  98.5 41.2 %copy-start.12 = (f32[2048,512]{1,0:T(8,128)S(1)}, f32[2048,512]{1,0:T(8,128)}, u32[]{:S(2)}) copy-start(f32[2048,512]{1,0:T(8,128)} %get-tuple-element.25) | copy-start | bytes 12582916
  139.7 3.7 %copy-start.11 = (f32[2048,512]{1,0:T(8,128)S(1)}, f32[2048,512]{1,0:T(8,128)}, u32[]{:S(2)}) copy-start(f32[2048,512]{1,0:T(8,128)} %get-tuple-element.26) | copy-start | bytes 12582916
  143.4 3.7 %copy-start.10 = (f32[512,2048]{1,0:T(8,128)S(1)}, f32[512,2048]{1,0:T(8,128)}, u32[]{:S(2)}) copy-start(f32[512,2048]{1,0:T(8,128)} %get-tuple-element.27) | copy-start | bytes 12582916

commit v3 on v2

--- a/solution.py
+++ b/solution.py
@@ -49,6 +49,15 @@
 
 GROUPS = 8
 BLOCKS = CHIPS // GROUPS
+UNITS = 8
+FIRST = (0, 0, 0, 1, 1, 1, 2, 2)
+UNIT_ORDER = (0, 3, 6, 1, 4, 7, 2, 5)
+PLANE = tuple(
+    sorted(
+        ((i, j) for i in range(SIDE) for j in range(SIDE) if i or j),
+        key=lambda p: -sum(min(a, SIDE - a) for a in p),
+    )
+)
 
 
 def greet_all(me, core):
@@ -83,11 +92,11 @@
 
 
 def experts_kernel(
-    routes,
-    weights,
-    stream,
-    gain,
-    cot,
+    routes_hbm,
+    weights_hbm,
+    stream_hbm,
+    gain_hbm,
+    cot_hbm,
     gate_hbm,
     up_hbm,
     down_hbm,
@@ -96,11 +105,15 @@
     gate_g,
     up_g,
     down_g,
+    routes,
+    weights,
+    stream,
+    gain,
+    cot,
     gate_w,
     up_w,
     down_w,
     square,
-    normed,
     select,
     send,
     rows_in,
@@ -109,7 +122,6 @@
     theirs,
     mine,
     other,
-    ret,
     back,
     load_sem,
     square_sem,
@@ -128,13 +140,22 @@
     half = stream.shape[1]
     depth = BLOCKS * capacity
     width = gate_w.shape[1]
-    barrier = greet_all(me, core)
-    loads = [
-        pltpu.make_async_copy(a, b, load_sem.at[i])
-        for i, (a, b) in enumerate(((gate_hbm, gate_w), (up_hbm, up_w), (down_hbm, down_w)))
-    ]
+    pairs = (
+        (stream_hbm, stream),
+        (gain_hbm, gain),
+        (routes_hbm, routes),
+        (weights_hbm, weights),
+        (cot_hbm, cot),
+        (gate_hbm, gate_w),
+        (up_hbm, up_w),
+        (down_hbm, down_w),
+    )
+    loads = [pltpu.make_async_copy(a, b, load_sem.at[i]) for i, (a, b) in enumerate(pairs)]
     for load in loads:
         load.start()
+    barrier = greet_all(me, core)
+    for load in loads[:5]:
+        load.wait()
     stream_float = stream[...].astype(jnp.float32)
     part = jnp.sum(stream_float * stream_float, axis=1, keepdims=True)
     square[0] = jnp.broadcast_to(part, square.shape[1:])
@@ -174,6 +195,7 @@
     swap.wait()
     inverse = lax.rsqrt((square[0, :, 0:1] + square[1, :, 0:1]) / D + EPSILON)
     inverse_out[...] = jnp.broadcast_to(inverse, inverse_out.shape)
+    normed = mine.at[pl.ds(0, tokens)]
     normed[...] = (stream_float * inverse * gain[...]).astype(jnp.bfloat16)
     for i, at in enumerate(range(0, CHIPS * capacity, chunk)):
         chosen = select[at : at + chunk]
@@ -195,7 +217,7 @@
             (peer, core),
         ).start()
     rows_in[core, (CHIPS - 1) * capacity :] = send[block(me)]
-    for load in loads:
+    for load in loads[5:]:
         load.wait()
 
     def group(g, count=depth):
@@ -207,7 +229,7 @@
 
     def exchange(g):
         return remote(
-            theirs.at[group(g)], other.at[group(g)], part_send.at[g], part_recv.at[g], partner
+            theirs.at[group(lax.rem(g, 2))], other.at[group(g)], part_send.at[g], part_recv.at[g], partner
         )
 
     def take(g):
@@ -242,16 +264,20 @@
         up_pre = (hidden_grad * silu_gate).astype(jnp.bfloat16)
         pre[rows, :width] = gate_pre
         pre[rows, width:] = up_pre
-        for target, side in ((theirs, 1 - core), (mine, core)):
+        pl.when(g >= 2)(lambda: exchange(g - 2).wait_send())
+        for target, at, side in (
+            (theirs, group(lax.rem(g, 2)), 1 - core),
+            (mine, rows, core),
+        ):
             features = pl.ds(pl.multiple_of(side * half, half), half)
             value = dot(gate_pre, gate_w[features], (1, 1)) + dot(up_pre, up_w[features], (1, 1))
-            target[rows] = value.astype(jnp.bfloat16)
+            target[at] = value.astype(jnp.bfloat16)
         exchange(g).start()
 
     def finish(g):
         wait_for(other.at[group(g)], part_recv.at[g])
         rows = group(g)
-        ret[rows] = (mine[rows].astype(jnp.float32) + other[rows].astype(jnp.float32)).astype(
+        mine[rows] = (mine[rows].astype(jnp.float32) + other[rows].astype(jnp.float32)).astype(
             jnp.bfloat16
         )
         for i in range(BLOCKS):
@@ -263,7 +289,7 @@
             y = lax.rem(lax.rem(me // 4, 4) + 4 - lax.rem(k // 4, 4), 4)
             x = lax.rem(lax.rem(me, 4) + 4 - lax.rem(k, 4), 4)
             go = remote(
-                ret.at[block(g * BLOCKS + i)],
+                mine.at[block(g * BLOCKS + i)],
                 back.at[block(me)],
                 back_send,
                 back_recv,
@@ -281,9 +307,9 @@
         return carry
 
     lax.fori_loop(0, GROUPS + 2, step, 0)
-    back[block(me)] = ret[(CHIPS - 1) * capacity :]
-
-    tile = 256
+    back[block(me)] = mine[(CHIPS - 1) * capacity :]
+
+    tile = 128
 
     def gate_step(i, carry):
         side, at = i // (half // tile), lax.rem(i, half // tile)
@@ -309,9 +335,10 @@
     wait_for(back.at[pl.ds(0, sent)], back_recv)
     normed_grad[...] = dot(select[...], back[...], (0, 0))
     wait_for(send.at[pl.ds(0, sent)], send_sem)
-    wait_for(ret.at[pl.ds(0, sent)], back_send)
+    wait_for(mine.at[pl.ds(0, sent)], back_send)
     for g in range(GROUPS):
         passing(g).wait_send()
+    for g in range(GROUPS - 2, GROUPS):
         exchange(g).wait_send()
 
 
@@ -320,7 +347,7 @@
     slots = 2 * tokens * routes.shape[0]
     width = gate_w.shape[1]
     vmem = pl.BlockSpec(memory_space=pltpu.VMEM)
-    hbm = pl.BlockSpec(memory_space=pl.ANY)
+    hbm = pl.BlockSpec(memory_space=pltpu.HBM)
     f32, bf16 = jnp.float32, jnp.bfloat16
     dma = pltpu.SemaphoreType.DMA
     return pl.pallas_call(
@@ -332,25 +359,28 @@
             jax.ShapeDtypeStruct((D, width), f32),
             jax.ShapeDtypeStruct((width, D), f32),
         ),
-        in_specs=[vmem] * 5 + [hbm] * 3,
+        in_specs=[hbm] * 8,
         out_specs=(vmem,) * 5,
         scratch_shapes=[
+            pltpu.VMEM(routes.shape, jnp.int32),
+            pltpu.VMEM(weights.shape, f32),
+            pltpu.VMEM((tokens, half), bf16),
+            pltpu.VMEM((1, half), f32),
+            pltpu.VMEM((tokens, half), bf16),
             pltpu.VMEM((D, width), bf16),
             pltpu.VMEM((D, width), bf16),
             pltpu.VMEM((width, D), bf16),
             pltpu.VMEM((2, tokens, 128), f32),
-            pltpu.VMEM((tokens, half), bf16),
             pltpu.VMEM((slots, tokens), bf16),
             pltpu.VMEM((slots, 2 * half), bf16),
             pltpu.VMEM((2, slots, 2 * half), bf16),
             pltpu.VMEM((slots, 2 * width), bf16),
             pltpu.VMEM((slots, width), bf16),
+            pltpu.VMEM((2 * slots // GROUPS, half), bf16),
             pltpu.VMEM((slots, half), bf16),
             pltpu.VMEM((slots, half), bf16),
             pltpu.VMEM((slots, half), bf16),
-            pltpu.VMEM((slots, half), bf16),
-            pltpu.VMEM((slots, half), bf16),
-            dma((3,)),
+            dma((8,)),
             dma((2,)),
             dma(()),
             dma((GROUPS,)),
@@ -362,10 +392,15 @@
             dma(()),
         ],
         compiler_params=pltpu.CompilerParams(
-            collective_id=0, has_side_effects=True, vmem_limit_bytes=60 << 20
+            collective_id=0, has_side_effects=True, vmem_limit_bytes=32 << 20
         ),
         name="experts",
-    )(routes, weights, stream, gain, cot, gate_w, up_w, down_w)
+    )(
+        *(
+            pltpu.with_memory_space_constraint(a, pltpu.HBM)
+            for a in (routes, weights, stream, gain, cot, gate_w, up_w, down_w)
+        )
+    )
 
 
 def tail_kernel(
@@ -392,12 +427,17 @@
     conv,
     delta,
     shares,
-    arrived,
+    got,
+    half_sum,
+    final,
     cross_sem,
     whole_sem,
     rim_sem,
     back_sem,
-    share_sem,
+    share_send,
+    share_recv,
+    sum_send,
+    sum_recv,
 ):
     me, core = lax.axis_index("sp"), lax.axis_index("tp")
     partner = (me, 1 - core)
@@ -448,47 +488,94 @@
     before = jnp.where(row == 0, older, jnp.where(row == 1, last, pltpu.roll(gated, 2, 0)))
     conv[...] = taps[0:1] * before + taps[1:2] * previous + taps[2:3] * gated
     mixer_out = (out_gate[...].astype(jnp.float32) * conv[...]).astype(jnp.bfloat16)
+
+    def split(side):
+        value = dot(whole[side], mixer_out, (0, 0)).astype(jnp.bfloat16)
+        value = value.reshape(2, SIDE, SIDE, 2, 16, value.shape[1])
+        for u in range(UNITS):
+            r, c = u // 4, u % 4
+            shares[u, pl.ds(side * 2, 2)] = value[:, :, :, r, :, c * 128 : (c + 1) * 128]
+
+    split(core)
     wait_for(whole.at[1 - core], whole_sem.at[1])
+    split(1 - core)
+    here = (me // 16, lax.rem(me // 4, 4), lax.rem(me, 4))
+
+    def at_place(place):
+        return (place[0] * 16 + place[1] * 4 + place[2], core)
+
+    def shifted(moves):
+        return [lax.rem(h + m, 4) for h, m in zip(here, moves)]
+
+    def plane(u, index):
+        first = FIRST[u]
+        return shares.at[(u,) + (slice(None),) * first + (index,)]
+
+    for u in UNIT_ORDER:
+        for i, step in enumerate((2, 1, 3)):
+            place = shifted([step if d == FIRST[u] else 0 for d in range(3)])
+            remote(
+                plane(u, place[FIRST[u]]),
+                got.at[u, i],
+                share_send,
+                share_recv.at[u],
+                at_place(place),
+            ).start()
     mixer_grad = dot(whole[0], out_proj[:half]) + dot(whole[1], out_proj[half:])
     delta[...] = mixer_grad * out_gate[...].astype(jnp.float32)
     rim_out[...] = delta[0:8]
     give = remote(rim_out, rim_back, back_sem.at[0], back_sem.at[1], (ahead, core))
-    for side in range(2):
-        shares[side * half : (side + 1) * half] = dot(whole[side], mixer_out, (0, 0)).astype(
-            jnp.bfloat16
-        )
+    bgate_grad[...] = (mixer_grad * conv[...]).astype(jnp.bfloat16)
     give.start()
-    height = proj_grad.shape[0]
-    for j, k in enumerate(ORDER):
-        peer = moved(me, k)
-        remote(
-            shares.at[pl.ds(pl.multiple_of(peer * height, height), height)],
-            arrived.at[j],
-            share_sem.at[0],
-            share_sem.at[1],
-            (peer, core),
-        ).start()
-    arrived[CHIPS - 1] = shares[pl.ds(pl.multiple_of(me * height, height), height)]
-    bgate_grad[...] = (mixer_grad * conv[...]).astype(jnp.bfloat16)
+
+    def spread(u):
+        rest = [d for d in range(3) if d != FIRST[u]]
+        for i, (one, two) in enumerate(PLANE):
+            moves = [0, 0, 0]
+            moves[rest[0]], moves[rest[1]] = one, two
+            place = shifted(moves)
+            remote(
+                half_sum.at[u, place[rest[0]], place[rest[1]]],
+                final.at[u, i],
+                sum_send,
+                sum_recv.at[u],
+                at_place(place),
+            ).start()
+
+    earlier = None
+    for u in UNIT_ORDER:
+        wait_for(got.at[u], share_recv.at[u])
+        value = plane(u, here[FIRST[u]])[...].astype(jnp.float32)
+        for i in range(SIDE - 1):
+            value = value + got[u, i].astype(jnp.float32)
+        half_sum[u] = value
+        if earlier is not None:
+            spread(earlier)
+        earlier = u
+    spread(earlier)
     give.wait()
     rim_delta = jnp.where(me == CHIPS - 1, jnp.zeros_like(rim_back[...]), rim_back[...])
     nearest, second = rim_delta[0:1], rim_delta[1:2]
-    here = delta[...]
-    following = jnp.where(row == tokens - 1, nearest, pltpu.roll(here, tokens - 1, 0))
+    change = delta[...]
+    following = jnp.where(row == tokens - 1, nearest, pltpu.roll(change, tokens - 1, 0))
     beyond = jnp.where(
         row == tokens - 2,
         nearest,
-        jnp.where(row == tokens - 1, second, pltpu.roll(here, tokens - 2, 0)),
-    )
-    gated_grad = taps[2:3] * here + taps[1:2] * following + taps[0:1] * beyond
+        jnp.where(row == tokens - 1, second, pltpu.roll(change, tokens - 2, 0)),
+    )
+    gated_grad = taps[2:3] * change + taps[1:2] * following + taps[0:1] * beyond
     input_grad[...] = (gated_grad * in_gate[...].astype(jnp.float32)).astype(jnp.bfloat16)
     cgate_grad[...] = (gated_grad * value_in[...].astype(jnp.float32)).astype(jnp.bfloat16)
-    wait_for(arrived.at[pl.ds(0, CHIPS - 1)], share_sem.at[1])
-    total = arrived[0].astype(jnp.float32)
-    for j in range(1, CHIPS):
-        total = total + arrived[j].astype(jnp.float32)
-    proj_grad[...] = total
-    wait_for(shares.at[pl.ds(0, (CHIPS - 1) * height)], share_sem.at[0])
+    for u in UNIT_ORDER:
+        rest = [d for d in range(3) if d != FIRST[u]]
+        wait_for(final.at[u], sum_recv.at[u])
+        total = half_sum[u, here[rest[0]], here[rest[1]]]
+        for i in range(len(PLANE)):
+            total = total + final[u, i]
+        r, c = u // 4, u % 4
+        proj_grad[r * 16 : (r + 1) * 16, c * 128 : (c + 1) * 128] = total
+    wait_for(got, share_send)
+    wait_for(final, sum_send)
     wait_for(whole.at[core], whole_sem.at[0])
 
 
@@ -518,19 +605,48 @@
             pltpu.VMEM((8, width), f32),
             pltpu.VMEM((tokens, width), f32),
             pltpu.VMEM((tokens, width), f32),
-            pltpu.VMEM((D, width), bf16),
-            pltpu.VMEM((CHIPS, height, width), bf16),
+            pltpu.VMEM((UNITS, SIDE, SIDE, SIDE, 16, 128), bf16),
+            pltpu.VMEM((UNITS, SIDE - 1, SIDE, SIDE, 16, 128), bf16),
+            pltpu.VMEM((UNITS, SIDE, SIDE, 16, 128), f32),
+            pltpu.VMEM((UNITS, len(PLANE), 16, 128), f32),
             dma((2,)),
             dma((2,)),
             dma((4,)),
             dma((2,)),
-            dma((2,)),
+            dma(()),
+            dma((UNITS,)),
+            dma(()),
+            dma((UNITS,)),
         ],
         compiler_params=pltpu.CompilerParams(
-            collective_id=1, has_side_effects=True, vmem_limit_bytes=24 << 20
+            collective_id=1, has_side_effects=True, vmem_limit_bytes=12 << 20
         ),
         name="tail",
     )(normed_grad, inverse, stream, gain, cot, value_in, out_gate, in_gate, taps, out_proj)
+
+
+def store_kernel(*refs):
+    count = len(refs) // 2
+    sem = refs[-1]
+    copies = [
+        pltpu.make_async_copy(refs[i], refs[count + i], sem.at[i]) for i in range(count)
+    ]
+    for copy in copies:
+        copy.start()
+    for copy in copies:
+        copy.wait()
+
+
+def store(*arrays):
+    return pl.pallas_call(
+        store_kernel,
+        out_shape=tuple(jax.ShapeDtypeStruct(a.shape, a.dtype) for a in arrays),
+        in_specs=[pl.BlockSpec(memory_space=pltpu.VMEM)] * len(arrays),
+        out_specs=(pl.BlockSpec(memory_space=pltpu.HBM),) * len(arrays),
+        scratch_shapes=[pltpu.SemaphoreType.DMA((len(arrays),))],
+        compiler_params=pltpu.CompilerParams(vmem_limit_bytes=1 << 20),
+        name="store",
+    )(*arrays)
 
 
 def local(
@@ -571,16 +687,10 @@
         conv_taps,
         out_proj,
     )
-    return (
-        stream_grad,
-        proj_grad,
-        input_grad,
-        bgate_grad,
-        cgate_grad,
-        gate_g[None],
-        up_g[None],
-        down_g[None],
-    )
+    outs = store(
+        stream_grad, proj_grad, input_grad, bgate_grad, cgate_grad, gate_g, up_g, down_g
+    )
+    return (*outs[:5], *(out[None] for out in outs[5:]))
 
 
 def solution(mesh):

time: 150 us -> 128 us (0.85)
  local copies, waits for them, and re-layouts: 15.1 us -> 0.03 us
  Pallas kernels: 133 us -> 126 us
    unnamed x34 -> x16, local copies, waits for them, and re-layouts: 15.1 us -> 0.03 us
    pallas_call x1, Pallas kernels: 37.7 us -> 31.4 us  [tail(): pl.pallas_call(tail_kernel, out_shape=(jax.ShapeDtypeStruct((tokens, half...]
    pallas_call x1, Pallas kernels: 95.5 us -> 89.8 us  [experts(): pl.pallas_call(experts_kernel, out_shape=(jax.ShapeDtypeStruct((tokens, h...]
    pallas_call x0 -> x1, Pallas kernels: none -> 5.18 us  [store(): pl.pallas_call(store_kernel, out_shape=tuple((jax.ShapeDtypeStruct(a.shap...]
where the time goes in v3:
time: 128 us; the launch traced here: 127 us
  Pallas kernels  126 us (98%)
    pallas_call x1, Pallas kernels, experts(): pl.pallas_call(experts_kernel, out_shape=(jax.ShapeDtypeStruct((tokens, h...  89.8 us
    pallas_call x1, Pallas kernels, tail(): pl.pallas_call(tail_kernel, out_shape=(jax.ShapeDtypeStruct((tokens, half...  31.4 us
    pallas_call x1, Pallas kernels, store(): pl.pallas_call(store_kernel, out_shape=tuple((jax.ShapeDtypeStruct(a.shap...  5.18 us

profile of v3, /device:TPU:0, one launch (start us, length us, event | category | flops | bytes accessed | tf_op | source)
XLA Modules:
  0.0 127.2 jit_solution(10724678171459659923)
XLA Ops:
  0.6 0.0 copy-start.1
  0.6 0.0 copy-start
  0.7 0.0 copy-start.2
  0.7 0.0 copy-start.7
  0.7 0.0 copy-start.5
  0.7 0.0 copy-start.4
  0.7 0.0 copy-start.3
  0.7 0.0 copy-start.6
  0.7 89.8 %experts.1 = (f32[256,1024]{1,0:T(8,128)S(1)}, f32[256,128]{1,0:T(8,128)S(1)}, f32[2048,512]{1,0:T(8,128)S(1)}, f32[2048,512]{1,0:T(8,128)S(1)}, f32[512,2048]{1,0:T(8,128)S(1)}) custom-call(s32[2,256]{1,0:T(2,128)} %bitcast.14, f32[2,256]{1,0:T(2,128)} %bitcast.15, bf16[256,1024]{1,0:T(8,128)(2,1)} %stream.1, f32[1,1024]{1,0:T(1,128)} %bitcast.9, ...), custom_call_target="tpu_custom_call" | custom-call | tf_op jit(solution)/shard_map/experts/pallas_call | solution.py:353
  90.5 0.0 copy-done.1
  90.5 0.0 copy-done
  90.5 0.0 copy-done.2
  90.6 0.0 copy-done.7
  90.6 0.0 copy-done.5
  90.6 0.0 copy-done.4
  90.6 0.0 copy-done.3
  90.6 0.0 copy-done.6
  90.6 31.4 %tail.1 = (bf16[256,1024]{1,0:T(8,128)(2,1)S(1)}, f32[32,512]{1,0:T(8,128)S(1)}, bf16[256,512]{1,0:T(8,128)(2,1)S(1)}, bf16[256,512]{1,0:T(8,128)(2,1)S(1)}, bf16[256,512]{1,0:T(8,128)(2,1)S(1)}) custom-call(f32[256,1024]{1,0:T(8,128)S(1)} %get-tuple-element.26.normed_grad, f32[256,128]{1,0:T(8,128)S(1)} %get-tuple-element.27.inverse_in, ...), custom_call_target="tpu_custom_call" | custom-call | tf_op jit(solution)/shard_map/tail/pallas_call | solution.py:589
  122.0 5.2 %store.1 = (bf16[256,1024]{1,0:T(8,128)(2,1)}, f32[32,512]{1,0:T(8,128)}, bf16[256,512]{1,0:T(8,128)(2,1)}, bf16[256,512]{1,0:T(8,128)(2,1)}, bf16[256,512]{1,0:...) custom-call(bf16[256,1024]{1,0:T(8,128)(2,1)S(1)} %get-tuple-element.28.refs_0_, ...), custom_call_target="tpu_custom_call" | custom-call | tf_op jit(solution)/shard_map/store/pallas_call | solution.py:641
Async XLA Ops:
  0.6 89.9 %copy-start.1 = (bf16[256,1024]{1,0:T(8,128)(2,1)S(1)}, bf16[256,1024]{1,0:T(8,128)(2,1)}, u32[]{:S(2)}) copy-start(bf16[256,1024]{1,0:T(8,128)(2,1)} %cot.1) | copy-start | bytes 1572868
  0.6 89.9 %copy-start = (bf16[256,1024]{1,0:T(8,128)(2,1)S(1)}, bf16[256,1024]{1,0:T(8,128)(2,1)}, u32[]{:S(2)}) copy-start(bf16[256,1024]{1,0:T(8,128)(2,1)} %stream.1) | copy-start | bytes 1572868
  0.7 89.9 %copy-start.2 = (bf16[2048,512]{1,0:T(8,128)(2,1)S(1)}, bf16[2048,512]{1,0:T(8,128)(2,1)}, u32[]{:S(2)}) copy-start(bf16[2048,512]{1,0:T(8,128)(2,1)} %out_proj.1) | copy-start | bytes 6291460
  0.7 89.9 %copy-start.7 = (f32[3,512]{1,0:T(4,128)S(1)}, f32[3,512]{1,0:T(4,128)}, u32[]{:S(2)}) copy-start(f32[3,512]{1,0:T(4,128)} %taps.1) | copy-start | bytes 18436
  0.7 89.9 %copy-start.5 = (bf16[256,512]{1,0:T(8,128)(2,1)S(1)}, bf16[256,512]{1,0:T(8,128)(2,1)}, u32[]{:S(2)}) copy-start(bf16[256,512]{1,0:T(8,128)(2,1)} %in_gate.1) | copy-start | bytes 786436
  0.7 89.9 %copy-start.4 = (bf16[256,512]{1,0:T(8,128)(2,1)S(1)}, bf16[256,512]{1,0:T(8,128)(2,1)}, u32[]{:S(2)}) copy-start(bf16[256,512]{1,0:T(8,128)(2,1)} %out_gate.1) | copy-start | bytes 786436
  0.7 89.9 %copy-start.3 = (bf16[256,512]{1,0:T(8,128)(2,1)S(1)}, bf16[256,512]{1,0:T(8,128)(2,1)}, u32[]{:S(2)}) copy-start(bf16[256,512]{1,0:T(8,128)(2,1)} %value_in.1) | copy-start | bytes 786436
  0.7 89.9 %copy-start.6 = (f32[1024]{0:T(1024)S(1)}, f32[1024]{0:T(1024)}, u32[]{:S(2)}) copy-start(f32[1024]{0:T(1024)} %param.14) | copy-start | bytes 12292

commit v4 on v3

--- a/solution.py
+++ b/solution.py
@@ -207,11 +207,13 @@
     def block(index):
         return pl.ds(pl.multiple_of(index * capacity, capacity), capacity)
 
-    for j, k in enumerate(ORDER):
-        peer = moved(me, k)
+    for i, k in enumerate(ORDER):
+        opposite = _join(*(-a for a in _parts(k)))
+        j = jnp.where(core == 0, i, ORDER.index(opposite))
+        peer = jnp.where(core == 0, moved(me, k), moved(me, opposite))
         remote(
             send.at[block(peer)],
-            rows_in.at[core, pl.ds(j * capacity, capacity)],
+            rows_in.at[core, block(j)],
             send_sem,
             recv_sem.at[j // BLOCKS],
             (peer, core),
@@ -302,11 +304,11 @@
 
     def step(i, carry):
         pl.when(i < GROUPS)(lambda: take(i))
-        pl.when((i >= 1) & (i <= GROUPS))(lambda: compute(i - 1))
-        pl.when(i >= 2)(lambda: finish(i - 2))
+        pl.when(i >= 1)(lambda: finish(i - 1))
+        pl.when(i < GROUPS)(lambda: compute(i))
         return carry
 
-    lax.fori_loop(0, GROUPS + 2, step, 0)
+    lax.fori_loop(0, GROUPS + 1, step, 0)
     back[block(me)] = mine[(CHIPS - 1) * capacity :]
 
     tile = 128

time: 128 us -> 128 us (level)
    pallas_call x1, Pallas kernels: 31.4 us -> 33.9 us  [tail(): pl.pallas_call(tail_kernel, out_shape=(jax.ShapeDtypeStruct((tokens, half...]
    pallas_call x1, Pallas kernels: 89.8 us -> 87.6 us  [experts(): pl.pallas_call(experts_kernel, out_shape=(jax.ShapeDtypeStruct((tokens, h...]
where the time goes in v4:
time: 128 us; the launch traced here: 127 us
  Pallas kernels  127 us (99%)
    pallas_call x1, Pallas kernels, experts(): pl.pallas_call(experts_kernel, out_shape=(jax.ShapeDtypeStruct((tokens, h...  87.6 us
    pallas_call x1, Pallas kernels, tail(): pl.pallas_call(tail_kernel, out_shape=(jax.ShapeDtypeStruct((tokens, half...  33.9 us
    pallas_call x1, Pallas kernels, store(): pl.pallas_call(store_kernel, out_shape=tuple((jax.ShapeDtypeStruct(a.shap...  5.18 us

profile of v4, /device:TPU:0, one launch (start us, length us, event | category | flops | bytes accessed | tf_op | source)
XLA Modules:
  0.0 127.5 jit_solution(3414268755819986883)
XLA Ops:
  0.6 0.0 copy-start.1
  0.6 0.0 copy-start
  0.7 0.0 copy-start.2
  0.7 0.0 copy-start.7
  0.7 0.0 copy-start.5
  0.7 0.0 copy-start.4
  0.7 0.0 copy-start.3
  0.7 0.0 copy-start.6
  0.7 87.6 %experts.1 = (f32[256,1024]{1,0:T(8,128)S(1)}, f32[256,128]{1,0:T(8,128)S(1)}, f32[2048,512]{1,0:T(8,128)S(1)}, f32[2048,512]{1,0:T(8,128)S(1)}, f32[512,2048]{1,0:T(8,128)S(1)}) custom-call(s32[2,256]{1,0:T(2,128)} %bitcast.14, f32[2,256]{1,0:T(2,128)} %bitcast.15, bf16[256,1024]{1,0:T(8,128)(2,1)} %stream.1, f32[1,1024]{1,0:T(1,128)} %bitcast.9, ...), custom_call_target="tpu_custom_call" | custom-call | tf_op jit(solution)/shard_map/experts/pallas_call | solution.py:355
  88.3 0.0 copy-done.1
  88.3 0.0 copy-done
  88.3 0.0 copy-done.2
  88.4 0.0 copy-done.7
  88.4 0.0 copy-done.5
  88.4 0.0 copy-done.4
  88.4 0.0 copy-done.3
  88.4 0.0 copy-done.6
  88.4 33.9 %tail.1 = (bf16[256,1024]{1,0:T(8,128)(2,1)S(1)}, f32[32,512]{1,0:T(8,128)S(1)}, bf16[256,512]{1,0:T(8,128)(2,1)S(1)}, bf16[256,512]{1,0:T(8,128)(2,1)S(1)}, bf16[256,512]{1,0:T(8,128)(2,1)S(1)}) custom-call(f32[256,1024]{1,0:T(8,128)S(1)} %get-tuple-element.26.normed_grad, f32[256,128]{1,0:T(8,128)S(1)} %get-tuple-element.27.inverse_in, ...), custom_call_target="tpu_custom_call" | custom-call | tf_op jit(solution)/shard_map/tail/pallas_call | solution.py:591
  122.3 5.2 %store.1 = (bf16[256,1024]{1,0:T(8,128)(2,1)}, f32[32,512]{1,0:T(8,128)}, bf16[256,512]{1,0:T(8,128)(2,1)}, bf16[256,512]{1,0:T(8,128)(2,1)}, bf16[256,512]{1,0:...) custom-call(bf16[256,1024]{1,0:T(8,128)(2,1)S(1)} %get-tuple-element.28.refs_0_, ...), custom_call_target="tpu_custom_call" | custom-call | tf_op jit(solution)/shard_map/store/pallas_call | solution.py:643
Async XLA Ops:
  0.6 87.7 %copy-start.1 = (bf16[256,1024]{1,0:T(8,128)(2,1)S(1)}, bf16[256,1024]{1,0:T(8,128)(2,1)}, u32[]{:S(2)}) copy-start(bf16[256,1024]{1,0:T(8,128)(2,1)} %cot.1) | copy-start | bytes 1572868
  0.6 87.7 %copy-start = (bf16[256,1024]{1,0:T(8,128)(2,1)S(1)}, bf16[256,1024]{1,0:T(8,128)(2,1)}, u32[]{:S(2)}) copy-start(bf16[256,1024]{1,0:T(8,128)(2,1)} %stream.1) | copy-start | bytes 1572868
  0.7 87.7 %copy-start.2 = (bf16[2048,512]{1,0:T(8,128)(2,1)S(1)}, bf16[2048,512]{1,0:T(8,128)(2,1)}, u32[]{:S(2)}) copy-start(bf16[2048,512]{1,0:T(8,128)(2,1)} %out_proj.1) | copy-start | bytes 6291460
  0.7 87.7 %copy-start.7 = (f32[3,512]{1,0:T(4,128)S(1)}, f32[3,512]{1,0:T(4,128)}, u32[]{:S(2)}) copy-start(f32[3,512]{1,0:T(4,128)} %taps.1) | copy-start | bytes 18436
  0.7 87.7 %copy-start.5 = (bf16[256,512]{1,0:T(8,128)(2,1)S(1)}, bf16[256,512]{1,0:T(8,128)(2,1)}, u32[]{:S(2)}) copy-start(bf16[256,512]{1,0:T(8,128)(2,1)} %in_gate.1) | copy-start | bytes 786436
  0.7 87.7 %copy-start.4 = (bf16[256,512]{1,0:T(8,128)(2,1)S(1)}, bf16[256,512]{1,0:T(8,128)(2,1)}, u32[]{:S(2)}) copy-start(bf16[256,512]{1,0:T(8,128)(2,1)} %out_gate.1) | copy-start | bytes 786436
  0.7 87.7 %copy-start.3 = (bf16[256,512]{1,0:T(8,128)(2,1)S(1)}, bf16[256,512]{1,0:T(8,128)(2,1)}, u32[]{:S(2)}) copy-start(bf16[256,512]{1,0:T(8,128)(2,1)} %value_in.1) | copy-start | bytes 786436
  0.7 87.7 %copy-start.6 = (f32[1024]{0:T(1024)S(1)}, f32[1024]{0:T(1024)}, u32[]{:S(2)}) copy-start(f32[1024]{0:T(1024)} %param.14) | copy-start | bytes 12292
